TPU v7x, 128 devices: a whole 4x4x4 slice. The times are simulated.
128 devices in a mesh: ep: 128 (over z, y, x, core).
Axes of the slice: x: 4, y: 4, z: 4, core: 2. Of those that a mesh axis runs over, the one named last changes fastest.
Arguments:
- tokens: bfloat16 [1024, 2048], P('ep'), may hold values from -6 to 6
- cache_keys: bfloat16 [1024, 1024, 128], P('ep'), may hold values from -80 to 80
- cache_values: bfloat16 [1024, 1024, 128], P('ep'), may hold values from -6 to 6
- cum_gates: float32 [1024, 1024, 2], P('ep'), may hold values from -1024 to 0, as said below
- lengths: int32 [1024], P('ep'), may hold values from 128 to 1024
- query_weight: bfloat16 [2048, 2048], replicated, may hold values from -0.125 to 0.125
- key_weight: bfloat16 [2048, 128], replicated, may hold values from -0.125 to 0.125
- value_weight: bfloat16 [2048, 128], replicated, may hold values from -0.125 to 0.125
- forget_weight: bfloat16 [2048, 2], replicated, may hold values from -0.125 to 0.125
- out_weight: bfloat16 [2048, 2048], P('ep'), may hold values from -1 to 1
- norm_gain: float32 [2, 2048], replicated, may hold values from 0.1 to 1.9
- norm_bias: float32 [2, 2048], replicated, may hold values from -1 to 1
- dense_gate_weight: bfloat16 [2048, 5632], P(None, 'ep'), may hold values from -0.125 to 0.125
- dense_up_weight: bfloat16 [2048, 5632], P(None, 'ep'), may hold values from -0.125 to 0.125
- dense_down_weight: bfloat16 [5632, 2048], P('ep'), may hold values from -0.078125 to 0.078125
- dense_scale: float32 [2048], replicated, may hold values from 0.2 to 1.5
- expert_gate_weight: bfloat16 [2048, 57344], P(None, 'ep'), may hold values from -0.125 to 0.125
- expert_up_weight: bfloat16 [2048, 57344], P(None, 'ep'), may hold values from -0.125 to 0.125
- expert_down_weight: bfloat16 [57344, 2048], P('ep'), may hold values from -0.0625 to 0.0625
- routes: int32 [1024, 2], replicated, may hold values from 0 to 7, all different within a row; in each aligned block of 8 rows (0 to 7, 8 to 15, ...) at most 3 rows name the same one
- route_weights: float32 [1024, 2], replicated, may hold values from 0.2 to 1
Outputs:
- output: bfloat16 [1024, 2048], P('ep')
Inputs may be any that keep to these rules, and one draw needn't show every extreme that they name: `routes`: each row names 2 different experts; the rows of one device (8 aligned rows) name one expert at most 3 times. `cum_gates`: non-increasing along positions.
All inputs are finite; a program needn't handle non-finite values.
Results may differ from a plain program's by a relative error of at most 0.012.
Values may be sent and summed in bfloat16 or wider, within the bound.
A program may use at most 128 MiB of HBM per device.

v0:
```python
import jax
import jax.numpy as jnp
from jax import lax
from jax.sharding import PartitionSpec as P

EXPERTS = 8
TOP = 2
CAP = 3


residual_scale = 1.4142135
norm_eps = 1e-05


def partner_2(block, axis, stride):
    count = lax.axis_size(axis)
    route = []
    for low in range(count):
        high = low | 1 << stride
        if high != low and high < count:
            route += [(low, high), (high, low)]
    return lax.ppermute(block, axis, route)


def layer_norm(values, gain_row, shift_row):
    centre = jnp.mean(values, axis=-1, keepdims=True)
    centred = values - centre
    spread = jnp.mean(centred * centred, axis=-1, keepdims=True)
    return (centred * lax.rsqrt(spread + norm_eps) * gain_row + shift_row).astype(jnp.bfloat16)


def attend(
    queries, cached_keys, cached_values, gate_sums, length_row, fresh_key, fresh_value, fresh_gate
):
    amount = queries.shape[0]
    cache_len = cached_keys.shape[1]
    kv_count = fresh_gate.shape[1]
    head_dim = fresh_key.shape[1] // kv_count
    grouped = queries.shape[1] // (kv_count * head_dim)
    query_grid_four = queries.reshape(amount, kv_count, grouped, head_dim)
    key_four = cached_keys.reshape(amount, cache_len, kv_count, head_dim)
    value_four = cached_values.reshape(amount, cache_len, kv_count, head_dim)
    self_key_row = fresh_key.reshape(amount, kv_count, head_dim)
    own_value = fresh_value.astype(jnp.float32).reshape(amount, kv_count, head_dim)
    ratio_value = head_dim ** (-0.5)
    latest = jnp.take_along_axis(gate_sums, (length_row - 1)[:, None, None], axis=1)
    offsets = jnp.transpose(latest - gate_sums + fresh_gate[:, None, :], (0, 2, 1))
    past = jnp.einsum(
        "bkgd,blkd->bkgl", query_grid_four, key_four, preferred_element_type=jnp.float32
    )
    past = past * ratio_value + offsets[:, :, None, :]
    live = jnp.arange(cache_len, dtype=jnp.int32)[None, :] < length_row[:, None]
    past = jnp.where(live[:, None, None, :], past, -jnp.inf)
    self_part = (
        jnp.einsum(
            "rifs,ris->rif", query_grid_four, self_key_row, preferred_element_type=jnp.float32
        )
        * ratio_value
    )
    highest = jnp.maximum(jnp.max(past, axis=-1), self_part)
    past_exp = jnp.exp(past - highest[..., None])
    own_exp = jnp.exp(self_part - highest)
    denominator = jnp.sum(past_exp, axis=-1) + own_exp
    past_weight = (past_exp / denominator[..., None]).astype(jnp.bfloat16)
    own_weight = (own_exp / denominator).astype(jnp.bfloat16)
    mixed = jnp.einsum(
        "bkgl,blkd->bkgd", past_weight, value_four, preferred_element_type=jnp.float32
    )
    mixed = mixed + own_weight.astype(jnp.float32)[..., None] * own_value[:, :, None, :]
    return mixed.reshape(amount, queries.shape[1]).astype(jnp.bfloat16)


def slot_tables(chosen, shares):
    expert_ids = jnp.arange(EXPERTS, dtype=jnp.int32)
    picked = (chosen[..., None] == expert_ids).astype(jnp.int32)
    hits = jnp.sum(picked, axis=2)
    portion = jnp.sum(picked.astype(jnp.float32) * shares[..., None], axis=2)
    ranks = jnp.cumsum(hits, axis=1) - hits
    slot_ids = jnp.arange(CAP, dtype=jnp.int32)
    matched = (hits[..., None] * (ranks[..., None] == slot_ids).astype(jnp.int32)).astype(
        jnp.float32
    )
    return (matched, portion)


def expert_part(inputs, gate_cols, up_cols, down_rows):
    gate_val = jnp.dot(inputs, gate_cols, preferred_element_type=jnp.float32)
    up_val = jnp.dot(inputs, up_cols, preferred_element_type=jnp.float32)
    hidden = (jax.nn.silu(gate_val) * up_val).astype(jnp.bfloat16)
    return jnp.dot(hidden, down_rows, preferred_element_type=jnp.float32).astype(jnp.bfloat16)


def experts_by_exchange(
    settled,
    routes,
    route_weights,
    own_index,
    shards,
    expert_gate_weight,
    expert_up_weight,
    expert_down_weight,
):
    rows_here = settled.shape[0]
    model_width = settled.shape[1]
    own_routes = lax.dynamic_slice_in_dim(routes, own_index * rows_here, rows_here, 0)
    own_shares = lax.dynamic_slice_in_dim(route_weights, own_index * rows_here, rows_here, 0)
    matched, portion = slot_tables(
        own_routes.reshape(1, rows_here, TOP), own_shares.reshape(1, rows_here, TOP)
    )
    matched = matched[0]
    portion = portion[0]
    send_slots = jnp.einsum(
        "sec,sd->ecd", matched.astype(jnp.bfloat16), settled, preferred_element_type=jnp.float32
    ).astype(jnp.bfloat16)
    outgoing = jnp.repeat(send_slots, shards, axis=0)
    received = lax.all_to_all(outgoing, "ep", split_axis=0, concat_axis=0, tiled=True)
    flat = received.reshape(-1, model_width)
    result = expert_part(flat, expert_gate_weight, expert_up_weight, expert_down_weight)
    answered = result.reshape(received.shape)
    returned = lax.all_to_all(answered, "ep", split_axis=0, concat_axis=0, tiled=True)
    summed = jnp.sum(
        returned.reshape(EXPERTS, shards, CAP, model_width).astype(jnp.float32), axis=1
    )
    return jnp.einsum("sec,ecd->sd", matched * portion[..., None], summed)


def local(
    tokens,
    cache_keys,
    cache_values,
    cum_gates,
    lengths,
    query_weight,
    key_weight,
    value_weight,
    forget_weight,
    out_weight,
    norm_gain,
    norm_bias,
    dense_gate_weight,
    dense_up_weight,
    dense_down_weight,
    dense_scale,
    expert_gate_weight,
    expert_up_weight,
    expert_down_weight,
    routes,
    route_weights,
):
    devices = lax.axis_size("ep")
    shards = devices // EXPERTS
    shard_bits = shards.bit_length() - 1
    total_bits = devices.bit_length() - 1
    own_index = lax.axis_index("ep")
    stacked = jnp.stack([dense_gate_weight, dense_up_weight, jnp.transpose(dense_down_weight)])
    for bit in range(shard_bits, total_bits):
        partner = partner_2(stacked, "ep", bit)
        upper = own_index >> bit & 1 == 1
        stacked = jnp.where(
            upper,
            jnp.concatenate([partner, stacked], axis=2),
            jnp.concatenate([stacked, partner], axis=2),
        )
    query = jnp.dot(tokens, query_weight, preferred_element_type=jnp.float32).astype(jnp.bfloat16)
    new_key = jnp.dot(tokens, key_weight, preferred_element_type=jnp.float32).astype(jnp.bfloat16)
    new_value = jnp.dot(tokens, value_weight, preferred_element_type=jnp.float32).astype(
        jnp.bfloat16
    )
    new_gate = jax.nn.log_sigmoid(
        jnp.dot(tokens, forget_weight, preferred_element_type=jnp.float32)
    )
    attended = attend(
        query, cache_keys, cache_values, cum_gates, lengths, new_key, new_value, new_gate
    )
    projected = jnp.dot(
        attended,
        lax.all_gather(out_weight, "ep", axis=0, tiled=True),
        preferred_element_type=jnp.float32,
    )
    settled = layer_norm(
        residual_scale * tokens.astype(jnp.float32) + projected, norm_gain[0], norm_bias[0]
    )
    group_rows = settled
    for bit in range(shard_bits):
        partner_rows = partner_2(group_rows, "ep", bit)
        upper = own_index >> bit & 1 == 1
        group_rows = jnp.where(
            upper,
            jnp.concatenate([partner_rows, group_rows], axis=0),
            jnp.concatenate([group_rows, partner_rows], axis=0),
        )
    dense_gate = jnp.dot(group_rows, stacked[0], preferred_element_type=jnp.float32)
    dense_up = jnp.dot(group_rows, stacked[1], preferred_element_type=jnp.float32)
    dense_hidden = (jax.nn.silu(dense_gate) * dense_up).astype(jnp.bfloat16)
    running = jnp.einsum("rf,df->rd", dense_hidden, stacked[2], preferred_element_type=jnp.float32)
    for bit in reversed(range(shard_bits)):
        half = running.shape[0] // 2
        upper = own_index >> bit & 1 == 1
        keep = jnp.where(upper, running[half:], running[:half])
        give = jnp.where(upper, running[:half], running[half:])
        running = keep + partner_2(give.astype(jnp.bfloat16), "ep", bit).astype(give.dtype)
    local_expert = experts_by_exchange(
        settled,
        routes,
        route_weights,
        own_index,
        shards,
        expert_gate_weight,
        expert_up_weight,
        expert_down_weight,
    )
    ffn = dense_scale * running + local_expert
    return layer_norm(
        residual_scale * settled.astype(jnp.float32) + ffn, norm_gain[1], norm_bias[1]
    )


def solution(mesh):
    return jax.shard_map(
        local,
        mesh=mesh,
        in_specs=(
            P("ep", None),
            P("ep", None, None),
            P("ep", None, None),
            P("ep", None, None),
            P("ep"),
            P(),
            P(),
            P(),
            P(),
            P("ep", None),
            P(),
            P(),
            P(None, "ep"),
            P(None, "ep"),
            P("ep", None),
            P(),
            P(None, "ep"),
            P(None, "ep"),
            P("ep", None),
            P(),
            P(),
        ),
        out_specs=P("ep", None),
        check_vma=False,
    )
```

profile of v0, /device:TPU:0, one launch (start us, length us, event | category | flops | bytes accessed | tf_op | source)
XLA Modules:
  0.0 263.8 jit_solution(18136717045035868061)
XLA Ops:
  6.5 0.7 all-gather.2.cloned.1.call-update
  7.3 1.2 pad_maximum_fusion
  8.5 3.4 %collective-permute-start.4 = (bf16[3,2048,44]{1,2,0:T(8,128)(2,1)S(1)}, bf16[3,2048,44]{1,2,0:T(8,128)(2,1)S(1)}, u32[]{:S(2)}, u32[]{:S(2)}) collective-permute-start(bf16[3,2048,44]{1,2,0:T(8,128)(2,1)S(1)} %pad_maximum_fusion), channel_id=1, source_target_pairs={{0,16},{16,0},{1,17},{17,1},{2,18},{18,2},{3,19},{19,3},{4,20},{20... | collective-permute-start | bytes 1622024 | tf_op jit(solution)/shard_map/ppermute | solution.py:22
  11.9 3.9 %copy.50 = bf16[8,1024,128]{1,2,0:T(8,128)(2,1)} copy(bf16[8,1024,128]{2,1,0:T(8,128)(2,1)} %param.23) | data formatting | bytes 4194304 | tf_op args[2]
  15.8 0.2 fusion.33
  15.9 0.1 copy.49
  16.0 2.6 copy.48
  18.6 4.6 %convolution_convert_fusion.2 = bf16[8,2048]{1,0:T(8,128)(2,1)S(1)} fusion(bf16[8,2048]{1,0:T(8,128)(2,1)S(1)} %copy-done.5, bf16[2048,2048]{1,0:T(8,128)(2,1)} %param.26), kind=kOutput, calls=%fused_computation.7 | convolution fusion | flops 67125248 | bytes 8454144 | tf_op jit(solution)/shard_map/dot_general | solution.py:164
  23.2 0.1 reshape.153
  23.4 3.9 %copy.47 = bf16[8,1024,128]{1,2,0:T(8,128)(2,1)} copy(bf16[8,1024,128]{2,1,0:T(8,128)(2,1)} %param.22) | data formatting | bytes 4194304 | tf_op args[1]
  27.3 1.2 convolution_convert_fusion.4
  28.5 0.1 reshape.176
  28.6 1.2 fusion.7
  29.8 0.1 reshape.160
  30.0 1.2 gather_fusion
  31.4 0.1 fusion.48
  31.5 0.1 add_bitcast_fusion
  31.7 2.1 fusion.46
  33.8 0.3 fusion.8
  34.2 0.4 maximum_select_fusion.2
  34.6 2.0 collective-permute-start.5
  36.6 0.7 fusion.6
  37.3 0.2 convert_element_type.123
  37.5 25.5 %collective-permute-done.5 = bf16[3,2048,88]{1,2,0:T(8,128)(2,1)} collective-permute-done((bf16[3,2048,88]{1,2,0:T(8,128)(2,1)S(1)}, bf16[3,2048,88]{1,2,0:T(8,128)(2,1)}, u32[]{:S(2)}, u32[]{:S(2)}) %collective-permute-start.5) | collective-permute-done | bytes 1081376 | tf_op jit(solution)/shard_map/ppermute | solution.py:22
  63.0 4.4 %maximum_select_fusion.1 = bf16[3,2048,176]{1,2,0:T(8,128)(2,1)} fusion(bf16[3,2048,88]{1,2,0:T(8,128)(2,1)S(1)} %maximum_select_fusion.2, bf16[3,2048,88]{1,2,0:T(8,128)(2,1)} %collective-permute-done.5, pred[]{:T(512)S(6)} %eq.71), kind=kLoop, calls=%fused_computation.8 | loop fusion | flops 9732096 | bytes 4325377 | tf_op jit(solution)/shard_map/jit(_where)/select_n | solution.py:159
  67.5 3.6 %collective-permute-start.6 = (bf16[3,2048,176]{1,2,0:T(8,128)(2,1)}, bf16[3,2048,176]{1,2,0:T(8,128)(2,1)}, u32[]{:S(2)}, u32[]{:S(2)}) collective-permute-start(bf16[3,2048,176]{1,2,0:T(8,128)(2,1)} %maximum_select_fusion.1), channel_id=1, source_target_pairs={{0,64},{64,0},{1,65},{65,1},{2,66},{66,2},{3,67},{67,3},{4,68},{68... | collective-permute-start | bytes 6488072 | tf_op jit(solution)/shard_map/ppermute | solution.py:22
  71.1 52.6 %all-gather.2.cloned.1.call-done = bf16[2048,2048]{1,0:T(8,128)(2,1)} async-done(((bf16[16,2048]{1,0:T(8,128)(2,1)}), bf16[2048,2048]{1,0:T(8,128)(2,1)}) %all-gather.2.cloned.1.call-update) | async-done | bytes 8388624 | tf_op jit(solution)/shard_map/all_gather | solution.py:177
  123.6 4.7 %fusion.47 = (f32[8]{0:T(128)S(1)}, f32[8,2048]{1,0:T(8,128)S(1)}) fusion(bf16[8,2048]{1,0:T(8,128)(2,1)S(1)} %convert_element_type.123, bf16[2048,2048]{1,0:T(8,128)(2,1)} %all-gather.2.cloned.1.call-done, bf16[8,2048]{1,0:T(8,128)(2,1)S(1)} %copy-done.5), kind=kOutput, calls=%fused_computation.107 | convolution fusion | flops 67174392 | bytes 8519712 | tf_op jit(solution)/shard_map/dot_general | solution.py:175
  128.3 0.2 multiply_reduce_fusion.1
  128.5 0.1 add_convert_fusion.1
  128.6 0.1 collective-permute-start
  128.7 1.2 collective-permute-done
  129.9 1.5 collective-permute-start.1
  131.5 2.8 %collective-permute-done.1 = bf16[16,2048]{1,0:T(8,128)(2,1)S(1)} collective-permute-done((bf16[16,2048]{1,0:T(8,128)(2,1)S(1)}, bf16[16,2048]{1,0:T(8,128)(2,1)S(1)}, u32[]{:S(2)}, u32[]{:S(2)}) %collective-permute-start.1) | collective-permute-done | bytes 65568 | tf_op jit(solution)/shard_map/ppermute | solution.py:22
  134.3 3.1 %collective-permute-start.2 = (bf16[32,2048]{1,0:T(8,128)(2,1)S(1)}, bf16[32,2048]{1,0:T(8,128)(2,1)S(1)}, u32[]{:S(2)}, u32[]{:S(2)}) collective-permute-start(bf16[32,2048]{1,0:T(8,128)(2,1)S(1)} %maximum_select_fusion.5), channel_id=1, source_target_pairs={{0,4},{4,0},{1,5},{5,1},{2,6},{6,2},{3,7},{7,3},{8,12},{12,8},{9,1... | collective-permute-start | bytes 393224 | tf_op jit(solution)/shard_map/ppermute | solution.py:22
  137.4 0.7 constant_dynamic-slice_fusion.1
  138.2 2.6 collective-permute-done.2
  140.9 1.0 collective-permute-start.3
  142.0 6.2 %maximum_select_fusion = bf16[3,2048,352]{1,2,0:T(8,128)(2,1)} fusion(bf16[3,2048,176]{1,2,0:T(8,128)(2,1)} %maximum_select_fusion.1, bf16[3,2048,176]{1,2,0:T(8,128)(2,1)} %collective-permute-done.6, pred[]{:T(512)S(6)} %eq.70), kind=kLoop, calls=%fused_computation.1 | loop fusion | flops 19464192 | bytes 8650753 | tf_op jit(solution)/shard_map/jit(_where)/select_n | solution.py:159
  148.1 0.2 convolution_convert_fusion.1
  148.3 0.1 copy.52
  148.4 2.4 broadcast_in_dim.21
  150.8 12.5 %all-to-all-start = ((bf16[128,3,2048]{2,1,0:T(4,128)(2,1)}), bf16[128,3,2048]{2,1,0:T(4,128)(2,1)}, u32[]{:S(2)}, u32[]{:S(2)}) async-start(bf16[128,3,2048]{2,1,0:T(4,128)(2,1)} %bitcast.66), calls=%async_computation | async-start | bytes 4194304 | tf_op jit(solution)/shard_map/all_to_all | solution.py:116
  163.3 0.7 copy-done.11
  164.0 2.6 fusion.1
  166.6 3.5 %fusion = f32[128,2048]{1,0:T(8,128)S(1)} fusion(bf16[3,2048,352]{1,2,0:T(8,128)(2,1)} %maximum_select_fusion, f32[128,352]{0,1:T(8,128)} %fusion.1, bf16[64,2048]{1,0:T(8,128)(2,1)S(1)} %maximum_select_fusion.4, bf16[64,2048]{1,0:T(8,128)(2,1)} %copy-done.11, pred[]{:T(512)S(6)} %eq.69), kind=kOutput, calls=%fused_computation.10 | convolution fusion | flops 371728384 | bytes 4636673 | tf_op jit(solution)/shard_map/rf,df->rd/dot_general | solution.py:195
  170.2 0.8 collective-permute-start.7
  171.0 0.7 constant_dynamic-slice_fusion
  171.7 20.2 %collective-permute-done.7 = bf16[64,2048]{1,0:T(8,128)(2,1)S(1)} collective-permute-done((bf16[64,2048]{1,0:T(8,128)(2,1)S(1)}, bf16[64,2048]{1,0:T(8,128)(2,1)S(1)}, u32[]{:S(2)}, u32[]{:S(2)}) %collective-permute-start.7) | collective-permute-done | bytes 262176 | tf_op jit(solution)/shard_map/ppermute | solution.py:22
  192.1 3.0 %collective-permute-start.8 = (bf16[32,2048]{1,0:T(8,128)(2,1)S(1)}, bf16[32,2048]{1,0:T(8,128)(2,1)S(1)}, u32[]{:S(2)}, u32[]{:S(2)}) collective-permute-start(bf16[32,2048]{1,0:T(8,128)(2,1)S(1)} %select_convert_fusion.1), channel_id=1, source_target_pairs={{0,4},{4,0},{1,5},{5,1},{2,6},{6,2},{3,7},{7,3},{8,12},{12,8},{9,1... | collective-permute-start | bytes 393224 | tf_op jit(solution)/shard_map/ppermute | solution.py:22
  195.1 5.0 %reshape.158 = bf16[384,2048]{1,0:T(8,128)(2,1)} reshape(bf16[128,3,2048]{2,1,0:T(4,128)(2,1)} %all-to-all-done) | data formatting | bytes 3145728 | tf_op jit(solution)/shard_map/reshape | solution.py:117
  200.1 3.1 %fusion.49 = f32[384,448]{0,1:T(8,128)S(1)} fusion(bf16[384,2048]{1,0:T(8,128)(2,1)} %reshape.158, bf16[2048,448]{0,1:T(8,128)(2,1)} %param.37), kind=kOutput, calls=%fused_computation.109 | convolution fusion | flops 704643072 | bytes 4096000 | tf_op jit(solution)/shard_map/dot_general | solution.py:87
  203.3 5.2 %convolution_convert_fusion = bf16[384,2048]{1,0:T(8,128)(2,1)} fusion(bf16[448,2048]{1,0:T(8,128)(2,1)S(1)} %copy-done, bf16[384,2048]{1,0:T(8,128)(2,1)} %reshape.158, bf16[2048,448]{0,1:T(8,128)(2,1)} %param.38, f32[384,448]{0,1:T(8,128)S(1)} %fusion.49), kind=kOutput, calls=%fused_computation.3 | convolution fusion | flops 1411104768 | bytes 7503872 | tf_op jit(solution)/shard_map/dot_general | solution.py:90
  208.5 5.1 %reshape.159 = bf16[128,3,2048]{2,1,0:T(4,128)(2,1)} reshape(bf16[384,2048]{1,0:T(8,128)(2,1)} %convolution_convert_fusion) | data formatting | bytes 3145728 | tf_op jit(solution)/shard_map/reshape | solution.py:119
  213.6 8.7 %all-to-all-start.1 = ((bf16[128,3,2048]{2,1,0:T(4,128)(2,1)}), bf16[128,3,2048]{2,1,0:T(4,128)(2,1)}, u32[]{:S(2)}, u32[]{:S(2)}) async-start(bf16[128,3,2048]{2,1,0:T(4,128)(2,1)} %reshape.159), calls=%async_computation.1 | async-start | bytes 4194304 | tf_op jit(solution)/shard_map/all_to_all | solution.py:120
  222.5 1.0 collective-permute-start.9
  223.5 23.5 %collective-permute-done.9 = bf16[16,2048]{1,0:T(8,128)(2,1)S(1)} collective-permute-done((bf16[16,2048]{1,0:T(8,128)(2,1)S(1)}, bf16[16,2048]{1,0:T(8,128)(2,1)S(1)}, u32[]{:S(2)}, u32[]{:S(2)}) %collective-permute-start.9) | collective-permute-done | bytes 65568 | tf_op jit(solution)/shard_map/ppermute | solution.py:22
  247.0 0.1 collective-permute-start.10
  247.1 5.8 %all-to-all-done.1 = bf16[128,3,2048]{2,1,0:T(4,128)(2,1)} async-done(((bf16[128,3,2048]{2,1,0:T(4,128)(2,1)}), bf16[128,3,2048]{2,1,0:T(4,128)(2,1)}, u32[]{:S(2)}, u32[]{:S(2)}) %all-to-all-start.1) | async-done | bytes 1572896 | tf_op jit(solution)/shard_map/all_to_all | solution.py:120
  252.9 2.7 %convert_reduce_fusion = bf16[8,3,2048]{2,1,0:T(4,128)(2,1)S(1)} fusion(bf16[128,3,2048]{2,1,0:T(4,128)(2,1)} %all-to-all-done.1), kind=kLoop, calls=%fused_computation.2 | loop fusion | flops 1523712 | bytes 1671168 | tf_op jit(solution)/shard_map/reduce_sum | solution.py:121
  255.6 0.2 convolution_bitcast_fusion
  255.8 0.2 fusion.43
  256.0 0.2 multiply_reduce_fusion
  256.2 0.7 add_convert_fusion
  (61 shorter events, 0.9 us)
Async XLA Ops:
  6.5 196.7 %copy-start = (bf16[448,2048]{1,0:T(8,128)(2,1)S(1)}, bf16[448,2048]{1,0:T(8,128)(2,1)}, u32[]{:S(2)}) copy-start(bf16[448,2048]{1,0:T(8,128)(2,1)} %param.39) | copy-start | bytes 5505028
  6.5 117.1 %all-gather.2.cloned.1.call-start = ((), (), s32[]{:S(2)}) async-start(), calls=%async_computation.2 | async-start | bytes 8454144 | tf_op jit(solution)/shard_map/all_gather | solution.py:177
  8.5 7.3 %copy-start.5 = (bf16[8,2048]{1,0:T(8,128)(2,1)S(1)}, bf16[8,2048]{1,0:T(8,128)(2,1)}, u32[]{:S(2)}) copy-start(bf16[8,2048]{1,0:T(8,128)(2,1)} %param.21) | copy-start | bytes 98308
  8.5 7.3 %copy-start.12 = (bf16[2048,2]{0,1:T(2,128)(2,1)S(1)}, bf16[2048,2]{0,1:T(2,128)(2,1)}, u32[]{:S(2)}) copy-start(bf16[2048,2]{0,1:T(2,128)(2,1)} %param.29) | copy-start | bytes 24580
  8.5 7.5 %copy-start.6 = (f32[8,1024,2]{1,2,0:T(2,128)S(1)}, f32[8,1024,2]{1,2,0:T(2,128)}, u32[]{:S(2)}) copy-start(f32[8,1024,2]{1,2,0:T(2,128)} %param.24) | copy-start | bytes 196612
  8.5 25.7 %collective-permute-start.4 = (bf16[3,2048,44]{1,2,0:T(8,128)(2,1)S(1)}, bf16[3,2048,44]{1,2,0:T(8,128)(2,1)S(1)}, u32[]{:S(2)}, u32[]{:S(2)}) collective-permute-start(bf16[3,2048,44]{1,2,0:T(8,128)(2,1)S(1)} %pad_maximum_fusion), channel_id=1, source_target_pairs={{0,16},{16,0},{1,17},{17,1},{2,18},{18,2},{3,19},{19,3},{4,20},{20... | collective-permute-start | bytes 1622024 | tf_op jit(solution)/shard_map/ppermute | solution.py:22
  23.3 6.6 %copy-start.10 = (s32[8]{0:T(128)S(1)}, s32[8]{0:T(128)}, u32[]{:S(2)}) copy-start(s32[8]{0:T(128)} %param.25) | copy-start | bytes 100
  31.6 2.6 copy-start.2
  31.6 2.6 copy-start.3
  31.7 2.6 copy-start.4
  33.8 2.8 %copy-start.1 = (bf16[8,1024,128]{1,2,0:T(8,128)(2,1)S(1)}, bf16[8,1024,128]{1,2,0:T(8,128)(2,1)}, u32[]{:S(2)}) copy-start(bf16[8,1024,128]{1,2,0:T(8,128)(2,1)} %copy.50) | copy-start | bytes 6291460
  34.6 28.4 %collective-permute-start.5 = (bf16[3,2048,88]{1,2,0:T(8,128)(2,1)S(1)}, bf16[3,2048,88]{1,2,0:T(8,128)(2,1)}, u32[]{:S(2)}, u32[]{:S(2)}) collective-permute-start(bf16[3,2048,88]{1,2,0:T(8,128)(2,1)S(1)} %maximum_select_fusion.2), channel_id=1, source_target_pairs={{0,32},{32,0},{1,33},{33,1},{2,34},{34,2},{3,35},{35,3},{4,36},{36... | collective-permute-start | bytes 3244040 | tf_op jit(solution)/shard_map/ppermute | solution.py:22
  36.6 0.9 copy-start.7
  36.6 0.9 copy-start.8
  67.5 74.5 %collective-permute-start.6 = (bf16[3,2048,176]{1,2,0:T(8,128)(2,1)}, bf16[3,2048,176]{1,2,0:T(8,128)(2,1)}, u32[]{:S(2)}, u32[]{:S(2)}) collective-permute-start(bf16[3,2048,176]{1,2,0:T(8,128)(2,1)} %maximum_select_fusion.1), channel_id=1, source_target_pairs={{0,64},{64,0},{1,65},{65,1},{2,66},{66,2},{3,67},{67,3},{4,68},{68... | collective-permute-start | bytes 6488072 | tf_op jit(solution)/shard_map/ppermute | solution.py:22
  128.6 1.3 collective-permute-start
  129.9 4.3 %collective-permute-start.1 = (bf16[16,2048]{1,0:T(8,128)(2,1)S(1)}, bf16[16,2048]{1,0:T(8,128)(2,1)S(1)}, u32[]{:S(2)}, u32[]{:S(2)}) collective-permute-start(bf16[16,2048]{1,0:T(8,128)(2,1)S(1)} %maximum_select_fusion.9), channel_id=1, source_target_pairs={{0,2},{2,0},{1,3},{3,1},{4,6},{6,4},{5,7},{7,5},{8,10},{10,8},{9,1... | collective-permute-start | bytes 196616 | tf_op jit(solution)/shard_map/ppermute | solution.py:22
  134.3 6.6 %collective-permute-start.2 = (bf16[32,2048]{1,0:T(8,128)(2,1)S(1)}, bf16[32,2048]{1,0:T(8,128)(2,1)S(1)}, u32[]{:S(2)}, u32[]{:S(2)}) collective-permute-start(bf16[32,2048]{1,0:T(8,128)(2,1)S(1)} %maximum_select_fusion.5), channel_id=1, source_target_pairs={{0,4},{4,0},{1,5},{5,1},{2,6},{6,2},{3,7},{7,3},{8,12},{12,8},{9,1... | collective-permute-start | bytes 393224 | tf_op jit(solution)/shard_map/ppermute | solution.py:22
  140.9 22.4 %collective-permute-start.3 = (bf16[64,2048]{1,0:T(8,128)(2,1)S(1)}, bf16[64,2048]{1,0:T(8,128)(2,1)S(1)}, u32[]{:S(2)}, u32[]{:S(2)}) collective-permute-start(bf16[64,2048]{1,0:T(8,128)(2,1)S(1)} %maximum_select_fusion.4), channel_id=1, source_target_pairs={{0,8},{8,0},{1,9},{9,1},{2,10},{10,2},{3,11},{11,3},{4,12},{12,4},... | collective-permute-start | bytes 786440 | tf_op jit(solution)/shard_map/ppermute | solution.py:22
  150.8 44.3 %all-to-all-start = ((bf16[128,3,2048]{2,1,0:T(4,128)(2,1)}), bf16[128,3,2048]{2,1,0:T(4,128)(2,1)}, u32[]{:S(2)}, u32[]{:S(2)}) async-start(bf16[128,3,2048]{2,1,0:T(4,128)(2,1)} %bitcast.66), calls=%async_computation | async-start | bytes 4194304 | tf_op jit(solution)/shard_map/all_to_all | solution.py:116
  163.3 0.7 copy-start.11
  170.2 21.8 %collective-permute-start.7 = (bf16[64,2048]{1,0:T(8,128)(2,1)S(1)}, bf16[64,2048]{1,0:T(8,128)(2,1)S(1)}, u32[]{:S(2)}, u32[]{:S(2)}) collective-permute-start(bf16[64,2048]{1,0:T(8,128)(2,1)S(1)} %select_convert_fusion), channel_id=1, source_target_pairs={{0,8},{8,0},{1,9},{9,1},{2,10},{10,2},{3,11},{11,3},{4,12},{12,4},... | collective-permute-start | bytes 786440 | tf_op jit(solution)/shard_map/ppermute | solution.py:22
  192.1 30.3 %collective-permute-start.8 = (bf16[32,2048]{1,0:T(8,128)(2,1)S(1)}, bf16[32,2048]{1,0:T(8,128)(2,1)S(1)}, u32[]{:S(2)}, u32[]{:S(2)}) collective-permute-start(bf16[32,2048]{1,0:T(8,128)(2,1)S(1)} %select_convert_fusion.1), channel_id=1, source_target_pairs={{0,4},{4,0},{1,5},{5,1},{2,6},{6,2},{3,7},{7,3},{8,12},{12,8},{9,1... | collective-permute-start | bytes 393224 | tf_op jit(solution)/shard_map/ppermute | solution.py:22
  213.6 39.2 %all-to-all-start.1 = ((bf16[128,3,2048]{2,1,0:T(4,128)(2,1)}), bf16[128,3,2048]{2,1,0:T(4,128)(2,1)}, u32[]{:S(2)}, u32[]{:S(2)}) async-start(bf16[128,3,2048]{2,1,0:T(4,128)(2,1)} %reshape.159), calls=%async_computation.1 | async-start | bytes 4194304 | tf_op jit(solution)/shard_map/all_to_all | solution.py:120
  222.4 33.4 %copy-start.9 = (f32[2048]{0:T(1024)S(1)}, f32[2048]{0:T(1024)}, u32[]{:S(2)}) copy-start(f32[2048]{0:T(1024)} %param.36) | copy-start | bytes 24580
  222.5 24.5 %collective-permute-start.9 = (bf16[16,2048]{1,0:T(8,128)(2,1)S(1)}, bf16[16,2048]{1,0:T(8,128)(2,1)S(1)}, u32[]{:S(2)}, u32[]{:S(2)}) collective-permute-start(bf16[16,2048]{1,0:T(8,128)(2,1)S(1)} %select_convert_fusion.2), channel_id=1, source_target_pairs={{0,2},{2,0},{1,3},{3,1},{4,6},{6,4},{5,7},{7,5},{8,10},{10,8},{9,1... | collective-permute-start | bytes 196616 | tf_op jit(solution)/shard_map/ppermute | solution.py:22
  247.0 8.8 %collective-permute-start.10 = (bf16[8,2048]{1,0:T(8,128)(2,1)S(1)}, bf16[8,2048]{1,0:T(8,128)(2,1)S(1)}, u32[]{:S(2)}, u32[]{:S(2)}) collective-permute-start(bf16[8,2048]{1,0:T(8,128)(2,1)S(1)} %select_convert_fusion.3), channel_id=1, source_target_pairs={{0,1},{1,0},{2,3},{3,2},{4,5},{5,4},{6,7},{7,6},{8,9},{9,8},{10,11... | collective-permute-start | bytes 98312 | tf_op jit(solution)/shard_map/ppermute | solution.py:22
Sparse Core Ops, SparseCore 0:
  10.3 113.2 all-gather.1
where the time goes:
time: 265 us; the launch traced here: 264 us
  waiting for transfers between devices  135 us (51%)
  starting transfers between devices  40.9 us (15%)
  matrix products  29.7 us (11%)
  local copies, waits for them, and re-layouts  27.2 us (10%)
  other arithmetic  17.4 us (7%)
  between operations  13.8 us (5%)
    ppermute x11, waiting for transfers between devices, partner_2(): return lax.ppermute(block, axis, route)  75.8 us
    all_gather x1, waiting for transfers between devices, local(): lax.all_gather(out_weight, 'ep', axis=0, tiled=True)  52.6 us
    ppermute x11, starting transfers between devices, partner_2(): return lax.ppermute(block, axis, route)  19.6 us
    all_to_all x1, starting transfers between devices, experts_by_exchange(): lax.all_to_all(outgoing, 'ep', split_axis=0, concat_axis=0, tiled=True)  12.5 us
    unnamed x30, local copies, waits for them, and re-layouts  11.2 us
    select_n x3, other arithmetic, local(): jnp.where(upper, jnp.concatenate([partner, stacked], axis=2), jnp.concate...  11 us
    all_to_all x1, starting transfers between devices, experts_by_exchange(): lax.all_to_all(answered, 'ep', split_axis=0, concat_axis=0, tiled=True)  8.75 us
    all_to_all x1, waiting for transfers between devices, experts_by_exchange(): lax.all_to_all(answered, 'ep', split_axis=0, concat_axis=0, tiled=True)  5.76 us
  transfers between devices with their start and end apart: 14, of which 8 were waited for; matrix products, arithmetic and copies ran while one was open for 27% of the time, Pallas kernels for 0%

commit v1 on v0

v1 whole, which is shorter than its diff:
```python
import functools

import jax
import jax.numpy as jnp
from jax import lax
from jax.experimental import pallas as pl
from jax.experimental.pallas import tpu as pltpu
from jax.sharding import PartitionSpec as P

N = 128
D = 2048
SEQ = 8
SLOTS = 1024
HID = 448
DEN = 44
HPAD = 512
residual_scale = 1.4142135
norm_eps = 1e-05
MESH = pl.DeviceIdType.MESH
NT = (((1,), (1,)), ((), ()))
F32 = jnp.float32
BF16 = jnp.bfloat16

COLOURS = ((0, 768, (2, 1, 0)), (768, 640, (0, 2, 1)), (1408, 640, (1, 0, 2)))


def layer_norm(values, gain_row, shift_row):
    centre = jnp.mean(values, axis=-1, keepdims=True)
    centred = values - centre
    spread = jnp.mean(centred * centred, axis=-1, keepdims=True)
    return (centred * lax.rsqrt(spread + norm_eps) * gain_row + shift_row).astype(BF16)


def remote(src, dst, send, recv, peer):
    return pltpu.make_async_remote_copy(
        src_ref=src, dst_ref=dst, send_sem=send, recv_sem=recv, device_id=(peer,), device_id_type=MESH
    )


def wait_bytes(ref, sem):
    pltpu.make_async_copy(ref, ref, sem).wait()


def attention_kernel(
    len_ref, tok_h, wq_h, wk_h, wv_h, fw_h, kc_h, vc_h, cg_h, ow_h, gain_h, bias_h,
    out_ref,
    tok, wq, wk, wv, fw, kc, vc, cg, ow, gain, bias,
    q3, o3, nk, nv, ng, wbuf, abuf, psend, prec,
    lsem, wsend, wrecv, asend, arecv, fsend, psem, rsem,
):
    me = lax.axis_index("ep")
    group = me // 16
    slot = lax.rem(me, 16)
    core = lax.rem(me, 2)
    partner = me + 1 - 2 * core
    barrier = pltpu.get_barrier_semaphore()

    def hello(i, carry):
        pl.semaphore_signal(barrier, inc=1, device_id=(lax.rem(me + i, N),), device_id_type=MESH)
        return carry

    lax.fori_loop(1, N, hello, 0)

    loads = {}

    def load(name, src, dst):
        loads[name] = pltpu.make_async_copy(src, dst, lsem.at[len(loads)])
        loads[name].start()

    load("tok", tok_h, tok)
    load("ow", ow_h, ow)
    for k in range(8):
        load(("wq", k), wq_h.at[pl.ds(k * 256, 256)], wq.at[pl.ds(k * 256, 256)])
    load("wk", wk_h, wk)
    load("wv", wv_h, wv)
    load("fw", fw_h, fw)
    load("cg", cg_h, cg)
    load("kc", kc_h, kc)
    load("vc", vc_h, vc)
    load("gain", gain_h, gain)
    load("bias", bias_h, bias)
    loads["tok"].wait()

    acc = jnp.zeros((SEQ, D), F32)
    for k in range(8):
        loads[("wq", k)].wait()
        acc = acc + jnp.dot(
            tok[:, k * 256:(k + 1) * 256], wq[k * 256:(k + 1) * 256, :], preferred_element_type=F32
        )
    acc = acc.astype(BF16).astype(F32)
    loads["wk"].wait()
    loads["wv"].wait()
    loads["fw"].wait()
    nk[...] = jnp.dot(tok[...], wk[...], preferred_element_type=F32).astype(BF16).astype(F32)
    nv[...] = jnp.dot(tok[...], wv[...], preferred_element_type=F32).astype(BF16).astype(F32)
    tok32 = tok[...].astype(F32)
    fw32 = fw[...].astype(F32)
    for j in range(2):
        x = jnp.sum(tok32 * fw32[j:j + 1, :], axis=-1, keepdims=True)
        gate = jnp.minimum(x, 0.0) - jnp.log1p(jnp.exp(-jnp.abs(x)))
        ng[j] = jnp.broadcast_to(gate, (SEQ, 128))

    lane = lax.broadcasted_iota(jnp.int32, (SEQ, 128), 1)
    for h in range(32):
        j = h // 16
        tile = acc[:, (h // 2) * 128:(h // 2 + 1) * 128]
        if h % 2 != j:
            tile = pltpu.roll(tile, 64, 1)
        keep = (lane < 64) if j == 0 else (lane >= 64)
        q3[h * 8:(h + 1) * 8, :] = jnp.where(keep, tile, 0.0)

    loads["ow"].wait()
    own_w = pltpu.make_async_copy(ow.at[:, pl.ds(pl.multiple_of(slot * 128, 128), 128)], wbuf.at[me], psem)
    own_w.start()
    pl.semaphore_wait(barrier, N - 1)
    loads["cg"].wait()
    loads["kc"].wait()
    loads["vc"].wait()
    pos = lax.broadcasted_iota(jnp.int32, (1, SLOTS), 1)

    def sequence(b, carry):
        def push(i, inner):
            off = b * 16 + i + 1

            @pl.when(off < N)
            def _():
                peer = lax.rem(me + off, N)
                column = pl.multiple_of(lax.rem(peer, 16) * 128, 128)
                remote(ow.at[:, pl.ds(column, 128)], wbuf.at[me], wsend, wrecv, peer).start()

            return inner

        lax.fori_loop(0, 16, push, 0)
        used = len_ref[b]
        qb = q3[pl.ds(b, 32, stride=8), :]
        s = lax.dot_general(qb.astype(BF16), kc[b], NT, preferred_element_type=F32)
        own = jnp.sum(qb * nk[pl.ds(b, 1), :], axis=-1, keepdims=True) * 0.125
        halves = []
        for j in range(2):
            sums = cg[b, j:j + 1, :]
            latest = jnp.sum(jnp.where(pos == used - 1, sums, 0.0), axis=-1, keepdims=True)
            offsets = latest - sums + ng[j, pl.ds(b, 1), :][:, 0:1]
            part = s[j * 16:(j + 1) * 16, :] * 0.125 + offsets
            halves.append(jnp.where(pos < used, part, -jnp.inf))
        s = jnp.concatenate(halves, axis=0)
        top = jnp.maximum(jnp.max(s, axis=-1, keepdims=True), own)
        e = jnp.exp(s - top)
        eo = jnp.exp(own - top)
        inv = 1.0 / (jnp.sum(e, axis=-1, keepdims=True) + eo)
        mixed = jnp.dot((e * inv).astype(BF16), vc[b], preferred_element_type=F32)
        mixed = mixed + (eo * inv).astype(BF16).astype(F32) * nv[pl.ds(b, 1), :]
        o3[pl.ds(b, 32, stride=8), :] = mixed
        return carry

    lax.fori_loop(0, SEQ, sequence, 0)
    for t in range(16):
        low = o3[(2 * t) * 8:(2 * t + 1) * 8, :]
        high = o3[(2 * t + 1) * 8:(2 * t + 2) * 8, :]
        if t < 8:
            high = pltpu.roll(high, 64, 1)
        else:
            low = pltpu.roll(low, 64, 1)
        abuf[slot, :, t * 128:(t + 1) * 128] = jnp.where(lane < 64, low, high).astype(BF16)

    sends = []
    for k in range(1, 8):
        other = lax.rem(slot + 2 * k, 16)
        copy = remote(abuf.at[slot], abuf.at[slot], asend.at[k], arecv.at[k], group * 16 + other)
        copy.start()
        sends.append(copy)
    copy = remote(abuf.at[slot], abuf.at[slot], fsend.at[0], arecv.at[8], partner)
    copy.start()
    sends.append(copy)
    for k in range(1, 8):
        source = lax.rem(slot + 16 - 2 * k, 16)
        wait_bytes(abuf.at[source], arecv.at[k])
        copy = remote(abuf.at[source], abuf.at[source], fsend.at[k], arecv.at[8 + k], partner)
        copy.start()
        sends.append(copy)
    for k in range(8):
        wait_bytes(abuf.at[slot], arecv.at[8 + k])
    own_w.wait()
    wait_bytes(wbuf.at[pl.ds(0, N - 1)], wrecv)

    product = jnp.dot(
        abuf[...].reshape(16 * SEQ, D), wbuf[...].reshape(D, 128), preferred_element_type=F32
    )
    psend[...] = product.reshape(16, SEQ, 128)
    for k in range(1, 16):
        other = lax.rem(slot + k, 16)
        remote(psend.at[other], prec.at[slot], rsem.at[0], rsem.at[1], group * 16 + other).start()
    prec[slot] = psend[slot]
    loads["gain"].wait()
    loads["bias"].wait()
    wait_bytes(prec.at[pl.ds(0, 15)], rsem.at[1])
    projected = jnp.concatenate([prec[k] for k in range(16)], axis=-1)
    out_ref[...] = layer_norm(residual_scale * tok32 + projected, gain[0:1, :], bias[0:1, :])
    for copy in sends:
        copy.wait_send()
    wait_bytes(psend.at[pl.ds(0, 15)], rsem.at[0])
    wait_bytes(wbuf.at[pl.ds(0, N - 1)], wsend)


def attention(tokens, keys, values, gates, lengths, qw, kw, vw, fw, ow, gain, bias):
    any_spec = pl.BlockSpec(memory_space=pl.ANY)
    return pl.pallas_call(
        attention_kernel,
        name="attention",
        out_shape=jax.ShapeDtypeStruct((SEQ, D), BF16),
        in_specs=[pl.BlockSpec(memory_space=pltpu.SMEM)] + [any_spec] * 11,
        out_specs=pl.BlockSpec(memory_space=pltpu.VMEM),
        scratch_shapes=[
            pltpu.VMEM((SEQ, D), BF16),
            pltpu.VMEM((D, D), BF16),
            pltpu.VMEM((D, 128), BF16),
            pltpu.VMEM((D, 128), BF16),
            pltpu.VMEM((2, D), BF16),
            pltpu.VMEM((SEQ, SLOTS, 128), BF16),
            pltpu.VMEM((SEQ, SLOTS, 128), BF16),
            pltpu.VMEM((SEQ, 2, SLOTS), F32),
            pltpu.VMEM((16, D), BF16),
            pltpu.VMEM((2, D), F32),
            pltpu.VMEM((2, D), F32),
            pltpu.VMEM((256, 128), F32),
            pltpu.VMEM((256, 128), F32),
            pltpu.VMEM((SEQ, 128), F32),
            pltpu.VMEM((SEQ, 128), F32),
            pltpu.VMEM((2, SEQ, 128), F32),
            pltpu.VMEM((N, 16, 128), BF16),
            pltpu.VMEM((16, SEQ, D), BF16),
            pltpu.VMEM((16, SEQ, 128), F32),
            pltpu.VMEM((16, SEQ, 128), F32),
            pltpu.SemaphoreType.DMA((18,)),
            pltpu.SemaphoreType.DMA,
            pltpu.SemaphoreType.DMA,
            pltpu.SemaphoreType.DMA((8,)),
            pltpu.SemaphoreType.DMA((16,)),
            pltpu.SemaphoreType.DMA((8,)),
            pltpu.SemaphoreType.DMA,
            pltpu.SemaphoreType.DMA((2,)),
        ],
        compiler_params=pltpu.CompilerParams(
            collective_id=0, has_side_effects=True, vmem_limit_bytes=60 * 1024 * 1024
        ),
    )(lengths, tokens, qw, kw, vw, fw, keys, values, gates, ow, gain, bias)


def ffn_kernel(
    settled, eg_h, eu_h, ed_h, dg_h, du_h, dd_h, scale, gain, bias, routes, shares,
    out_ref,
    full, wg, wu, wd, dg, du, dd, hid, portion, part, crec, chip, r1, t1, r2, t2, r3,
    lsem, gsend, grecv, fsend, frecv, csend, crecv, ssend, srecv,
):
    me = lax.axis_index("ep")
    core = lax.rem(me, 2)
    partner = me + 1 - 2 * core
    place = (me // 32, lax.rem(me // 8, 4), lax.rem(me // 2, 4))
    stride = (32, 8, 2)

    def peer_at(axis, d):
        return me + (lax.rem(place[axis] + d, 4) - place[axis]) * stride[axis]

    barrier = pltpu.get_barrier_semaphore()
    peers = [partner] + [peer_at(axis, d) for axis in range(3) for d in (1, 2, 3)]
    for peer in peers:
        pl.semaphore_signal(barrier, inc=1, device_id=(peer,), device_id_type=MESH)

    loads = [
        pltpu.make_async_copy(src, dst, lsem.at[i])
        for i, (src, dst) in enumerate(
            [
                (eg_h, wg.at[pl.ds(0, HID)]),
                (eu_h, wu.at[pl.ds(0, HID)]),
                (ed_h, wd.at[pl.ds(0, HID)]),
                (dg_h, dg),
                (du_h, du),
                (dd_h, dd),
            ]
        )
    ]
    for copy in loads:
        copy.start()
    full[place[0], place[1], place[2], core] = settled[...]
    pl.semaphore_wait(barrier, len(peers))

    def slab(ref, fixed, colour, middle=()):
        start, width, _ = COLOURS[colour]
        index = [slice(None)] * 3
        for axis, value in fixed.items():
            index[axis] = value
        return ref.at[(*index, *middle, slice(None), pl.ds(start, width))]

    sends = []

    def gather_phase(colour, phase):
        order = COLOURS[colour][2]
        axis = order[phase]
        fixed = {a: place[a] for a in order[phase:]}
        for d in (1, 2, 3):
            view = slab(full, fixed, colour, (core,))
            copy = remote(
                view, view, gsend.at[colour, phase, d - 1], grecv.at[colour, phase, d - 1], peer_at(axis, d)
            )
            copy.start()
            sends.append(copy)

    def gather_wait(colour, phase, d):
        order = COLOURS[colour][2]
        axis = order[phase]
        fixed = {a: place[a] for a in order[phase:]}
        fixed[axis] = lax.rem(place[axis] + 4 - d, 4)
        view = slab(full, fixed, colour, (core,))
        wait_bytes(view, grecv.at[colour, phase, d - 1])
        return fixed

    def forward(colour, fixed, number):
        view = slab(full, fixed, colour, (core,))
        copy = remote(view, view, fsend.at[colour, number], frecv.at[colour, number], partner)
        copy.start()
        sends.append(copy)

    for colour in range(3):
        gather_phase(colour, 0)

    expert = me // 16
    share_row = jnp.sum(jnp.where(routes[...] == expert, shares[...], 0.0), axis=0, keepdims=True)
    for i in range(8):
        square = jnp.broadcast_to(share_row[:, i * 128:(i + 1) * 128], (128, 128))
        portion[i * 128:(i + 1) * 128, :] = square.T

    for colour in range(3):
        for d in (1, 2, 3):
            gather_wait(colour, 0, d)
        gather_phase(colour, 1)
    for copy in loads:
        copy.wait()
    for ref, extra in ((wg, dg), (wu, du)):
        ref[480:HPAD, :] = jnp.zeros((HPAD - 480, D), BF16)
        ref[HID:HID + DEN, :] = extra[...]
    wd[480:HPAD, :] = jnp.zeros((HPAD - 480, D), BF16)
    wd[HID:HID + DEN, :] = (dd[...].astype(F32) * scale[...]).astype(BF16)
    for colour in range(3):
        for d in (1, 2, 3):
            gather_wait(colour, 1, d)
        gather_phase(colour, 2)
        last = COLOURS[colour][2][2]
        forward(colour, {last: place[last]}, 0)
    for d in (1, 3, 2):
        for colour in range(3):
            forward(colour, gather_wait(colour, 2, d), d)
    for colour in range(3):
        last = COLOURS[colour][2][2]
        for d in range(4):
            view = slab(full, {last: 0}, colour, (0,))
            wait_bytes(view, frecv.at[colour, d])

    column = lax.broadcasted_iota(jnp.int32, (256, HPAD), 1)

    def hidden(z, carry):
        rows = full[z].reshape(256, D)
        gate = lax.dot_general(rows, wg[...], NT, preferred_element_type=F32)
        up = lax.dot_general(rows, wu[...], NT, preferred_element_type=F32)
        weight = portion[pl.ds(pl.multiple_of(z * 256, 256), 256), :]
        weight = jnp.concatenate([weight] * 4, axis=1)
        value = gate / (1.0 + jnp.exp(-gate)) * up
        value = jnp.where(column < HID, value * weight, value)
        hid[pl.ds(pl.multiple_of(z * 256, 256), 256), :] = value.astype(BF16)
        return carry

    lax.fori_loop(0, 4, hidden, 0)

    def scatter_phase(colour, phase):
        order = COLOURS[colour][2]
        axis = order[2 - phase]
        source = (chip, t1, t2)[phase]
        target = (r1, r2, r3)[phase]
        for d in (1, 2, 3):
            view = slab(source, {a: lax.rem(place[a] + d, 4) if a == axis else 0 if phase and a in order[3 - phase:] else slice(None) for a in range(3)}, colour)
            land = slab(target.at[d - 1], {a: 0 if a in order[2 - phase:] else slice(None) for a in range(3)}, colour)
            copy = remote(
                view, land, ssend.at[colour, phase, d - 1], srecv.at[colour, phase, d - 1], peer_at(axis, d)
            )
            copy.start()
            sends.append(copy)

    return_values = []

    def scatter_sum(colour, phase):
        order = COLOURS[colour][2]
        axis = order[2 - phase]
        source = (chip, t1, t2)[phase]
        target = (r1, r2, r3)[phase]
        own = slab(source, {a: place[a] if a == axis else 0 if phase and a in order[3 - phase:] else slice(None) for a in range(3)}, colour)
        total = own[...].astype(F32)
        for d in (1, 3, 2):
            land = slab(target.at[d - 1], {a: 0 if a in order[2 - phase:] else slice(None) for a in range(3)}, colour)
            wait_bytes(land, srecv.at[colour, phase, d - 1])
            total = total + land[...].astype(F32)
        if phase < 2:
            keep = slab((t1, t2)[phase], {a: 0 if a in order[2 - phase:] else slice(None) for a in range(3)}, colour)
            keep[...] = total.astype(BF16)
        return total

    for colour in range(3):
        start, width, _ = COLOURS[colour]

        def down(z, carry, start=start, width=width):
            block = hid[pl.ds(pl.multiple_of(z * 256, 256), 256), :]
            value = jnp.dot(block, wd[:, start:start + width], preferred_element_type=F32)
            part[z, :, :, :, :, start:start + width] = value.astype(BF16).reshape(4, 4, 2, SEQ, width)
            return carry

        lax.fori_loop(0, 4, down, 0)
        copies = []
        view = part.at[:, :, :, 1 - core, :, pl.ds(start, width)]
        land = crec.at[:, :, :, :, pl.ds(start, width)]
        copy = remote(view, land, csend.at[colour], crecv.at[colour], partner)
        copy.start()
        sends.append(copy)
        copy.wait_recv()

        def join(z, carry, start=start, width=width):
            value = part[z, :, :, core, :, start:start + width].astype(F32)
            value = value + crec[z, :, :, :, start:start + width].astype(F32)
            chip[z, :, :, :, start:start + width] = value.astype(BF16)
            return carry

        lax.fori_loop(0, 4, join, 0)
        scatter_phase(colour, 0)
    for phase in (0, 1):
        for colour in range(3):
            scatter_sum(colour, phase)
            scatter_phase(colour, phase + 1)
    pieces = [scatter_sum(colour, 2) for colour in range(3)]
    ffn = jnp.concatenate(pieces, axis=-1)
    base = residual_scale * settled[...].astype(F32)
    out_ref[...] = layer_norm(base + ffn, gain[1:2, :], bias[1:2, :])
    for copy in sends:
        copy.wait_send()


def ffn(settled, eg, eu, ed, dg, du, dd, scale, gain, bias, routes, shares):
    any_spec = pl.BlockSpec(memory_space=pl.ANY)
    vmem = pl.BlockSpec(memory_space=pltpu.VMEM)
    return pl.pallas_call(
        ffn_kernel,
        name="ffn",
        out_shape=jax.ShapeDtypeStruct((SEQ, D), BF16),
        in_specs=[vmem] + [any_spec] * 6 + [vmem] * 5,
        out_specs=vmem,
        scratch_shapes=[
            pltpu.VMEM((4, 4, 4, 2, SEQ, D), BF16),
            pltpu.VMEM((HPAD, D), BF16),
            pltpu.VMEM((HPAD, D), BF16),
            pltpu.VMEM((HPAD, D), BF16),
            pltpu.VMEM((DEN, D), BF16),
            pltpu.VMEM((DEN, D), BF16),
            pltpu.VMEM((DEN, D), BF16),
            pltpu.VMEM((N * SEQ, HPAD), BF16),
            pltpu.VMEM((N * SEQ, 128), F32),
            pltpu.VMEM((4, 4, 4, 2, SEQ, D), BF16),
            pltpu.VMEM((4, 4, 4, SEQ, D), BF16),
            pltpu.VMEM((4, 4, 4, SEQ, D), BF16),
            pltpu.VMEM((3, 4, 4, 4, SEQ, D), BF16),
            pltpu.VMEM((4, 4, 4, SEQ, D), BF16),
            pltpu.VMEM((3, 4, 4, 4, SEQ, D), BF16),
            pltpu.VMEM((4, 4, 4, SEQ, D), BF16),
            pltpu.VMEM((3, 4, 4, 4, SEQ, D), BF16),
            pltpu.SemaphoreType.DMA((6,)),
            pltpu.SemaphoreType.DMA((3, 3, 3)),
            pltpu.SemaphoreType.DMA((3, 3, 3)),
            pltpu.SemaphoreType.DMA((3, 4)),
            pltpu.SemaphoreType.DMA((3, 4)),
            pltpu.SemaphoreType.DMA((3,)),
            pltpu.SemaphoreType.DMA((3,)),
            pltpu.SemaphoreType.DMA((3, 3, 3)),
            pltpu.SemaphoreType.DMA((3, 3, 3)),
        ],
        compiler_params=pltpu.CompilerParams(
            collective_id=1, has_side_effects=True, vmem_limit_bytes=60 * 1024 * 1024
        ),
    )(settled, eg, eu, ed, dg, du, dd, scale, gain, bias, routes, shares)


def local(
    tokens, cache_keys, cache_values, cum_gates, lengths, query_weight, key_weight, value_weight,
    forget_weight, out_weight, norm_gain, norm_bias, dense_gate_weight, dense_up_weight,
    dense_down_weight, dense_scale, expert_gate_weight, expert_up_weight, expert_down_weight,
    routes, route_weights,
):
    settled = attention(
        tokens, cache_keys, cache_values, jnp.transpose(cum_gates, (0, 2, 1)), lengths, query_weight,
        key_weight, value_weight, forget_weight.T, out_weight, norm_gain, norm_bias,
    )
    return ffn(
        settled, expert_gate_weight.T, expert_up_weight.T, expert_down_weight, dense_gate_weight.T,
        dense_up_weight.T, dense_down_weight, dense_scale.reshape(1, D), norm_gain, norm_bias,
        routes.T, route_weights.T,
    )


def solution(mesh):
    return jax.shard_map(
        local,
        mesh=mesh,
        in_specs=(
            P("ep", None), P("ep", None, None), P("ep", None, None), P("ep", None, None), P("ep"),
            P(), P(), P(), P(), P("ep", None), P(), P(), P(None, "ep"), P(None, "ep"), P("ep", None),
            P(), P(None, "ep"), P(None, "ep"), P("ep", None), P(), P(),
        ),
        out_specs=P("ep", None),
        check_vma=False,
    )
```

time: 265 us -> 88.3 us (0.33)
  waiting for transfers between devices: 135 us -> 0 us
  Pallas kernels: 0 us -> 86.6 us
  starting transfers between devices: 40.9 us -> 0 us
  matrix products: 29.7 us -> 0 us
  local copies, waits for them, and re-layouts: 27.2 us -> 1.38 us
  other arithmetic: 17.4 us -> 0 us
  between operations: 13.8 us -> 0.02 us
    pallas_call x0 -> x2, Pallas kernels: none -> 86.6 us  [the longest x1 58.1 us: ffn(): pl.pallas_call(ffn_kernel, name='ffn', out_shape=jax.ShapeDtypeStruct((SE...]
    ppermute x11 -> x0, waiting for transfers between devices: 75.8 us -> none  [partner_2(): return lax.ppermute(block, axis, route)]
    all_gather x1 -> x0, waiting for transfers between devices: 52.6 us -> none  [local(): lax.all_gather(out_weight, 'ep', axis=0, tiled=True)]
    dot_general x14 -> x0, matrix products: 29.7 us -> none  [the longest x1 5.23 us: expert_part(): jnp.dot(hidden, down_rows, preferred_element_type=jnp.float32)]
    all_to_all x2 -> x0, starting transfers between devices: 21.2 us -> none  [the longest x1 12.5 us: experts_by_exchange(): lax.all_to_all(outgoing, 'ep', split_axis=0, concat_axis=0, tiled=True)]
    ppermute x11 -> x0, starting transfers between devices: 19.6 us -> none  [partner_2(): return lax.ppermute(block, axis, route)]
    select_n x8 -> x0, other arithmetic: 11.1 us -> none  [the longest x3 11 us: local(): jnp.where(upper, jnp.concatenate([partner, stacked], axis=2), jnp.concate...]
    reshape x4 -> x0, local copies, waits for them, and re-layouts: 10.4 us -> none  [the longest x1 5.15 us: experts_by_exchange(): answered = result.reshape(received.shape)]
  transfers between devices with their start and end apart: 14 -> 0, of which waited for: 8 -> 0; matrix products, arithmetic and copies ran while one was open for 27% -> 0% of each run, Pallas kernels for 0% -> 0%
where the time goes in v1:
time: 88.3 us; the launch traced here: 88 us
  Pallas kernels  86.6 us (98%)
  local copies, waits for them, and re-layouts  1.38 us (2%)
    pallas_call x1, Pallas kernels, ffn(): pl.pallas_call(ffn_kernel, name='ffn', out_shape=jax.ShapeDtypeStruct((SE...  58.1 us
    pallas_call x1, Pallas kernels, attention(): pl.pallas_call(attention_kernel, name='attention', out_shape=jax.ShapeDty...  28.5 us

profile of v1, /device:TPU:0, one launch (start us, length us, event | category | flops | bytes accessed | tf_op | source)
XLA Modules:
  0.0 88.0 jit_solution(9594732855827495506)
XLA Ops:
  0.0 28.5 %attention.1.settled = bf16[8,2048]{1,0:T(8,128)(2,1)} custom-call(s32[8]{0:T(128)} %len_ref.1, bf16[8,2048]{1,0:T(8,128)(2,1)} %tok_h.1, bf16[2048,2048]{1,0:T(8,128)(2,1)} %wq_h.1, bf16[2048,128]{1,0:T(8,128)(2,1)} %wk_h.1, bf16[2048,128]{1,0:T(8,128)(2,1)} %wv_h.1, bf16[2,2048]{1,0:T(2,128)(2,1)} %bitcast.14, bf16[8,1024,128]{2,1,0:T(8,128)(2,1)} %kc_h.1, ...), custom_call_target="tpu_custom_call" | custom-call | tf_op jit(solution)/shard_map/attention/pallas_call | solution.py:206
  28.5 58.1 %ffn.1 = bf16[8,2048]{1,0:T(8,128)(2,1)} custom-call(bf16[8,2048]{1,0:T(8,128)(2,1)} %attention.1.settled, bf16[448,2048]{1,0:T(8,128)(2,1)} %bitcast.9, bf16[448,2048]{1,0:T(8,128)(2,1)} %bitcast.10, bf16[448,2048]{1,0:T(8,128)(2,1)} %ed_h.1, bf16[44,2048]{1,0:T(8,128)(2,1)} %bitcast.11, bf16[44,2048]{1,0:T(8,128)(2,1)} %bitcast.12, bf16[44,2048]{1,0:T(8,128)(2,1)} %dd_h.1, ...), custom_call_target="tpu_custom_call" | custom-call | tf_op jit(solution)/shard_map/ffn/pallas_call | solution.py:445
  86.6 1.4 %copy.23 = bf16[8,2048]{1,0:T(8,128)(2,1)} copy(bf16[8,2048]{1,0:T(8,128)(2,1)} %ffn.1) | data formatting | bytes 65536

commit v2 on v1

v2 whole, which is shorter than its diff:
```python
import functools

import jax
import jax.numpy as jnp
from jax import lax
from jax.experimental import pallas as pl
from jax.experimental.pallas import tpu as pltpu
from jax.sharding import PartitionSpec as P

N = 128
D = 2048
SEQ = 8
SLOTS = 1024
HID = 448
DEN = 44
HPAD = 512
residual_scale = 1.4142135
norm_eps = 1e-05
MESH = pl.DeviceIdType.MESH
NT = (((1,), (1,)), ((), ()))
F32 = jnp.float32
BF16 = jnp.bfloat16

COLOURS = ((0, 768, (2, 1, 0)), (768, 640, (0, 2, 1)), (1408, 640, (1, 0, 2)))


def layer_norm(values, gain_row, shift_row):
    centre = jnp.mean(values, axis=-1, keepdims=True)
    centred = values - centre
    spread = jnp.mean(centred * centred, axis=-1, keepdims=True)
    return (centred * lax.rsqrt(spread + norm_eps) * gain_row + shift_row).astype(BF16)


def remote(src, dst, send, recv, peer):
    return pltpu.make_async_remote_copy(
        src_ref=src, dst_ref=dst, send_sem=send, recv_sem=recv, device_id=(peer,), device_id_type=MESH
    )


def wait_bytes(ref, sem):
    pltpu.make_async_copy(ref, ref, sem).wait()


def step_kernel(
    len_ref, tok_h, wq_h, wk_h, wv_h, fw_h, kc_h, vc_h, cg_h, ow_h, gain_h, bias_h,
    eg_h, eu_h, ed_h, dg_h, du_h, dd_h, scale_h, routes_h, shares_h,
    out_ref,
    tok, wq, wk, wv, fw, kc, vc, cg, ow, gain, bias,
    q3, o3, nk, nv, ng, wbuf, abuf, psend, prec,
    full, wgu, wd, dg, du, dd, scale, routes, shares, portion, acc, hid,
    part, crec, chip, r1, t1, r2, t2, r3,
    lsem, esem, wsend, wrecv, asend, arecv, fwsend, psem, rsem,
    gsend, grecv, fsend, frecv, csend, crecv, s1send, s1recv, s2send, s2recv, s3send, s3recv,
):
    me = lax.axis_index("ep")
    group = me // 16
    slot = lax.rem(me, 16)
    core = lax.rem(me, 2)
    partner = me + 1 - 2 * core
    place = (me // 32, lax.rem(me // 8, 4), lax.rem(me // 2, 4))
    stride = (32, 8, 2)

    def peer_at(axis, d):
        return me + (lax.rem(place[axis] + d, 4) - place[axis]) * stride[axis]

    loads = {}

    def load(name, src, dst):
        loads[name] = pltpu.make_async_copy(src, dst, lsem.at[len(loads)])
        loads[name].start()

    load("tok", tok_h, tok)
    for k in range(8):
        load(("wq", k), wq_h.at[pl.ds(k * 256, 256)], wq.at[pl.ds(k * 256, 256)])
    load("ow", ow_h, ow)
    load("wk", wk_h, wk)
    load("wv", wv_h, wv)
    load("fw", fw_h, fw)
    load("cg", cg_h, cg)
    load("kc", kc_h, kc)
    load("vc", vc_h, vc)

    barrier = pltpu.get_barrier_semaphore()

    def hello(i, carry):
        pl.semaphore_signal(barrier, inc=1, device_id=(lax.rem(me + i, N),), device_id_type=MESH)
        return carry

    lax.fori_loop(1, N, hello, 0)
    later = []
    for src, dst in (
        (gain_h, gain), (bias_h, bias), (eg_h, wgu.at[pl.ds(0, HID)]), (eu_h, wgu.at[pl.ds(HPAD, HID)]),
        (ed_h, wd.at[pl.ds(0, HID)]), (dg_h, dg), (du_h, du), (dd_h, dd), (scale_h, scale),
        (routes_h, routes), (shares_h, shares),
    ):
        copy = pltpu.make_async_copy(src, dst, esem.at[len(later)])
        copy.start()
        later.append(copy)
    loads["tok"].wait()

    q = jnp.zeros((SEQ, D), F32)
    for k in range(8):
        loads[("wq", k)].wait()
        q = q + jnp.dot(
            tok[:, k * 256:(k + 1) * 256], wq[k * 256:(k + 1) * 256, :], preferred_element_type=F32
        )
    q = q.astype(BF16).astype(F32)
    loads["wk"].wait()
    loads["wv"].wait()
    loads["fw"].wait()
    nk[...] = jnp.dot(tok[...], wk[...], preferred_element_type=F32).astype(BF16).astype(F32)
    nv[...] = jnp.dot(tok[...], wv[...], preferred_element_type=F32).astype(BF16).astype(F32)
    tok32 = tok[...].astype(F32)
    fw32 = fw[...].astype(F32)
    for j in range(2):
        x = jnp.sum(tok32 * fw32[j:j + 1, :], axis=-1, keepdims=True)
        gate = jnp.minimum(x, 0.0) - jnp.log1p(jnp.exp(-jnp.abs(x)))
        ng[j] = jnp.broadcast_to(gate, (SEQ, 128))

    lane = lax.broadcasted_iota(jnp.int32, (SEQ, 128), 1)
    for h in range(32):
        j = h // 16
        tile = q[:, (h // 2) * 128:(h // 2 + 1) * 128]
        if h % 2 != j:
            tile = pltpu.roll(tile, 64, 1)
        keep = (lane < 64) if j == 0 else (lane >= 64)
        q3[h * 8:(h + 1) * 8, :] = jnp.where(keep, tile, 0.0)

    loads["ow"].wait()
    own_w = pltpu.make_async_copy(ow.at[:, pl.ds(pl.multiple_of(slot * 128, 128), 128)], wbuf.at[me], psem)
    own_w.start()
    loads["cg"].wait()
    loads["kc"].wait()
    loads["vc"].wait()
    pos = lax.broadcasted_iota(jnp.int32, (1, SLOTS), 1)

    def sequence(b, carry):
        used = len_ref[b]
        qb = q3[pl.ds(b, 32, stride=8), :]
        s = lax.dot_general(qb.astype(BF16), kc[b], NT, preferred_element_type=F32)
        own = jnp.sum(qb * nk[pl.ds(b, 1), :], axis=-1, keepdims=True) * 0.125
        halves = []
        for j in range(2):
            sums = cg[b, j:j + 1, :]
            latest = jnp.sum(jnp.where(pos == used - 1, sums, 0.0), axis=-1, keepdims=True)
            offsets = latest - sums + ng[j, pl.ds(b, 1), :][:, 0:1]
            scores = s[j * 16:(j + 1) * 16, :] * 0.125 + offsets
            halves.append(jnp.where(pos < used, scores, -jnp.inf))
        s = jnp.concatenate(halves, axis=0)
        top = jnp.maximum(jnp.max(s, axis=-1, keepdims=True), own)
        e = jnp.exp(s - top)
        eo = jnp.exp(own - top)
        inv = 1.0 / (jnp.sum(e, axis=-1, keepdims=True) + eo)
        mixed = jnp.dot((e * inv).astype(BF16), vc[b], preferred_element_type=F32)
        mixed = mixed + (eo * inv).astype(BF16).astype(F32) * nv[pl.ds(b, 1), :]
        o3[pl.ds(b, 32, stride=8), :] = mixed
        return carry

    lax.fori_loop(0, SEQ, sequence, 0)
    for t in range(16):
        low = o3[(2 * t) * 8:(2 * t + 1) * 8, :]
        high = o3[(2 * t + 1) * 8:(2 * t + 2) * 8, :]
        if t < 8:
            high = pltpu.roll(high, 64, 1)
        else:
            low = pltpu.roll(low, 64, 1)
        abuf[slot, :, t * 128:(t + 1) * 128] = jnp.where(lane < 64, low, high).astype(BF16)

    pl.semaphore_wait(barrier, N - 1)
    sends = []
    for k in range(1, 8):
        other = lax.rem(slot + 2 * k, 16)
        copy = remote(abuf.at[slot], abuf.at[slot], asend.at[k], arecv.at[k], group * 16 + other)
        copy.start()
        sends.append(copy)
    copy = remote(abuf.at[slot], abuf.at[slot], fwsend.at[0], arecv.at[8], partner)
    copy.start()
    sends.append(copy)

    def push(i, carry):
        peer = lax.rem(me + i, N)
        column = pl.multiple_of(lax.rem(peer, 16) * 128, 128)
        remote(ow.at[:, pl.ds(column, 128)], wbuf.at[me], wsend, wrecv, peer).start()
        return carry

    lax.fori_loop(1, N, push, 0)

    for copy in later:
        copy.wait()
    expert = me // 16
    share_row = jnp.sum(jnp.where(routes[...] == expert, shares[...], 0.0), axis=0, keepdims=True)
    for i in range(8):
        square = jnp.broadcast_to(share_row[:, i * 128:(i + 1) * 128], (128, 128))
        portion[i * 128:(i + 1) * 128, :] = square.T
    for base, extra in ((0, dg), (HPAD, du)):
        wgu[base + 480:base + HPAD, :] = jnp.zeros((HPAD - 480, D), BF16)
        wgu[base + HID:base + HID + DEN, :] = extra[...]
    wd[480:HPAD, :] = jnp.zeros((HPAD - 480, D), BF16)
    wd[HID:HID + DEN, :] = (dd[...].astype(F32) * scale[...]).astype(BF16)

    def clear(z, carry):
        acc[z] = jnp.zeros((4, 4, 2, SEQ, 2 * HPAD), F32)
        return carry

    lax.fori_loop(0, 4, clear, 0)

    for k in range(1, 8):
        source = lax.rem(slot + 16 - 2 * k, 16)
        wait_bytes(abuf.at[source], arecv.at[k])
        copy = remote(abuf.at[source], abuf.at[source], fwsend.at[k], arecv.at[8 + k], partner)
        copy.start()
        sends.append(copy)
    for k in range(8):
        wait_bytes(abuf.at[slot], arecv.at[8 + k])
    own_w.wait()
    wait_bytes(wbuf.at[pl.ds(0, N - 1)], wrecv)

    product = jnp.dot(
        abuf[...].reshape(16 * SEQ, D), wbuf[...].reshape(D, 128), preferred_element_type=F32
    )
    psend[...] = product.reshape(16, SEQ, 128)
    for k in range(1, 16):
        other = lax.rem(slot + k, 16)
        remote(psend.at[other], prec.at[slot], rsem.at[0], rsem.at[1], group * 16 + other).start()
    prec[slot] = psend[slot]
    wait_bytes(prec.at[pl.ds(0, 15)], rsem.at[1])
    projected = jnp.concatenate([prec[k] for k in range(16)], axis=-1)
    full[place[0], place[1], place[2], core] = layer_norm(
        residual_scale * tok32 + projected, gain[0:1, :], bias[0:1, :]
    )

    def cut(ref, fixed, colour, middle=(), wide=False):
        start, width, _ = COLOURS[colour]
        index = [fixed.get(axis, slice(None)) for axis in range(3)]
        columns = slice(None) if wide else pl.ds(start, width)
        return ref.at[(*index, *middle, slice(None), columns)]

    def gather_send(colour, phase, fixed):
        axis = COLOURS[colour][2][phase]
        view = cut(full, fixed, colour, (core,))
        for d in (2, 1, 3):
            remote(view, view, gsend.at[colour, phase], grecv.at[colour, phase, d - 1], peer_at(axis, d)).start()

    def gather_wait(colour, phase, d):
        order = COLOURS[colour][2]
        fixed = {a: place[a] for a in order[phase:]}
        fixed[order[phase]] = lax.rem(place[order[phase]] + 4 - d, 4)
        wait_bytes(cut(full, fixed, colour, (core,)), grecv.at[colour, phase, d - 1])
        return fixed

    def forward(colour, fixed, number):
        view = cut(full, fixed, colour, (core,))
        remote(view, view, fsend.at[colour], frecv.at[colour, number], partner).start()

    everything = dict(enumerate(place))
    for phase in range(3):
        for colour in range(3):
            gather_send(colour, phase, everything)
    for d in (1, 3, 2):
        for colour in range(3):
            fixed = gather_wait(colour, 0, d)
            gather_send(colour, 1, fixed)
            gather_send(colour, 2, fixed)
    for d in (1, 3, 2):
        for colour in range(3):
            fixed = gather_wait(colour, 1, d)
            gather_send(colour, 2, fixed)
    for colour in range(3):
        last = COLOURS[colour][2][2]
        forward(colour, {last: place[last]}, 0)

    def gate_up(i, carry):
        @pl.when(i == 1)
        def _():
            for number, d in ((1, 1), (2, 3)):
                for colour in range(3):
                    forward(colour, {COLOURS[colour][2][2]: gather_wait(colour, 2, d)[COLOURS[colour][2][2]]}, number)

        @pl.when(i == 2)
        def _():
            for colour in range(3):
                forward(colour, {COLOURS[colour][2][2]: gather_wait(colour, 2, 2)[COLOURS[colour][2][2]]}, 3)

        d = i + (i // 2) * (5 - 2 * i)
        for colour in range(3):
            start, width, order = COLOURS[colour]
            fixed = {order[2]: lax.rem(place[order[2]] + 4 - d, 4)}
            wait_bytes(cut(full, fixed, colour, (0,)), frecv.at[colour, i])
            rows = cut(full, fixed, colour, (slice(None),))[...].reshape(256, width)
            value = lax.dot_general(rows, wgu[:, start:start + width], NT, preferred_element_type=F32)
            total = cut(acc, fixed, colour, (slice(None),), wide=True)
            total[...] = total[...] + value.reshape(4, 4, 2, SEQ, 2 * HPAD)
        return carry

    lax.fori_loop(0, 4, gate_up, 0)

    column = lax.broadcasted_iota(jnp.int32, (256, HPAD), 1)

    def activate(z, carry):
        both = acc[z].reshape(256, 2 * HPAD)
        gate, up = both[:, :HPAD], both[:, HPAD:]
        weight = portion[pl.ds(pl.multiple_of(z * 256, 256), 256), :]
        weight = jnp.concatenate([weight] * 4, axis=1)
        value = gate / (1.0 + jnp.exp(-gate)) * up
        value = jnp.where(column < HID, value * weight, value)
        hid[z] = value.astype(BF16).reshape(4, 4, 2, SEQ, HPAD)
        return carry

    lax.fori_loop(0, 4, activate, 0)

    def turn(i):
        return 2 - i + (i // 2) * (7 - 2 * i)

    def scatter(i, carry):
        @pl.when(i < 4)
        def _():
            for colour in range(3):
                start, width, order = COLOURS[colour]
                fixed = {order[2]: lax.rem(place[order[2]] + turn(i), 4)}
                rows = cut(hid, fixed, colour, (slice(None),), wide=True)[...].reshape(256, HPAD)
                value = jnp.dot(rows, wd[:, start:start + width], preferred_element_type=F32)
                cut(part, fixed, colour, (slice(None),))[...] = value.astype(BF16).reshape(4, 4, 2, SEQ, width)
                remote(
                    cut(part, fixed, colour, (1 - core,)), cut(crec, fixed, colour),
                    csend.at[colour], crecv.at[colour, i], partner,
                ).start()

        @pl.when(i > 0)
        def _():
            d = turn(i - 1)
            for colour in range(3):
                order = COLOURS[colour][2]
                v3 = lax.rem(place[order[2]] + d, 4)
                fixed = {order[2]: v3}
                wait_bytes(cut(crec, fixed, colour), crecv.at[colour, i - 1])
                total = cut(part, fixed, colour, (core,))[...].astype(F32) + cut(crec, fixed, colour)[...].astype(F32)
                cut(chip, fixed, colour)[...] = total.astype(BF16)

                @pl.when(i < 4)
                def _():
                    start, width, _ = COLOURS[colour]
                    for d2 in (2, 1, 3, 0):
                        v2 = lax.rem(place[order[1]] + d2, 4)
                        remote(
                            cut(chip, {order[2]: v3, order[1]: v2}, colour),
                            r1.at[d - 1, v2, :, :, pl.ds(start, width)],
                            s1send.at[colour], s1recv.at[colour, d - 1, d2], peer_at(order[2], d),
                        ).start()

        return carry

    lax.fori_loop(0, 5, scatter, 0)

    for d2 in (2, 1, 3, 0):
        for colour in range(3):
            start, width, order = COLOURS[colour]
            columns = pl.ds(start, width)
            v2 = lax.rem(place[order[1]] + d2, 4)
            total = cut(chip, {order[2]: place[order[2]], order[1]: v2}, colour)[...].astype(F32)
            for d in (2, 1, 3):
                land = r1.at[d - 1, v2, :, :, columns]
                wait_bytes(land, s1recv.at[colour, d - 1, d2])
                total = total + land[...].astype(F32)
            t1[v2, :, :, start:start + width] = total.astype(BF16)
            if d2:
                remote(
                    t1.at[v2, :, :, columns], r2.at[d2 - 1, :, :, columns],
                    s2send.at[colour, d2 - 1], s2recv.at[colour, d2 - 1], peer_at(order[1], d2),
                ).start()
    for colour in range(3):
        start, width, order = COLOURS[colour]
        columns = pl.ds(start, width)
        total = t1[place[order[1]], :, :, start:start + width].astype(F32)
        for d in (1, 3, 2):
            land = r2.at[d - 1, :, :, columns]
            wait_bytes(land, s2recv.at[colour, d - 1])
            total = total + land[...].astype(F32)
        t2[:, :, start:start + width] = total.astype(BF16)
        for d in (2, 1, 3):
            remote(
                t2.at[lax.rem(place[order[0]] + d, 4), :, columns], r3.at[d - 1, :, columns],
                s3send.at[colour, d - 1], s3recv.at[colour, d - 1], peer_at(order[0], d),
            ).start()
    pieces = []
    for colour in range(3):
        start, width, order = COLOURS[colour]
        total = t2[place[order[0]], :, start:start + width].astype(F32)
        for d in (1, 3, 2):
            land = r3.at[d - 1, :, pl.ds(start, width)]
            wait_bytes(land, s3recv.at[colour, d - 1])
            total = total + land[...].astype(F32)
        pieces.append(total)
    base = residual_scale * full[place[0], place[1], place[2], core].astype(F32)
    out_ref[...] = layer_norm(base + jnp.concatenate(pieces, axis=-1), gain[1:2, :], bias[1:2, :])

    for copy in sends:
        copy.wait_send()
    wait_bytes(psend.at[pl.ds(0, 15)], rsem.at[0])
    wait_bytes(wbuf.at[pl.ds(0, N - 1)], wsend)
    for colour in range(3):
        start, width, order = COLOURS[colour]
        columns = pl.ds(start, width)
        wait_bytes(full.at[0, 0, pl.ds(0, 3), 0, :, columns], gsend.at[colour, 0])
        wait_bytes(full.at[0, pl.ds(0, 3), :, 0, :, columns], gsend.at[colour, 1])
        wait_bytes(full.at[pl.ds(0, 3), :, :, 0, :, columns], gsend.at[colour, 2])
        wait_bytes(full.at[:, :, :, 0, :, columns], fsend.at[colour])
        wait_bytes(crec.at[:, :, :, :, columns], csend.at[colour])
        wait_bytes(r1.at[:, :, :, :, columns], s1send.at[colour])
        for d in range(3):
            wait_bytes(r2.at[d, :, :, columns], s2send.at[colour, d])
            wait_bytes(r3.at[d, :, columns], s3send.at[colour, d])


def step(*operands):
    any_spec = pl.BlockSpec(memory_space=pl.ANY)
    dma = pltpu.SemaphoreType.DMA
    return pl.pallas_call(
        step_kernel,
        name="step",
        out_shape=jax.ShapeDtypeStruct((SEQ, D), BF16),
        in_specs=[pl.BlockSpec(memory_space=pltpu.SMEM)] + [any_spec] * 20,
        out_specs=pl.BlockSpec(memory_space=pltpu.VMEM),
        scratch_shapes=[
            pltpu.VMEM((SEQ, D), BF16),
            pltpu.VMEM((D, D), BF16),
            pltpu.VMEM((D, 128), BF16),
            pltpu.VMEM((D, 128), BF16),
            pltpu.VMEM((2, D), BF16),
            pltpu.VMEM((SEQ, SLOTS, 128), BF16),
            pltpu.VMEM((SEQ, SLOTS, 128), BF16),
            pltpu.VMEM((SEQ, 2, SLOTS), F32),
            pltpu.VMEM((16, D), BF16),
            pltpu.VMEM((2, D), F32),
            pltpu.VMEM((2, D), F32),
            pltpu.VMEM((256, 128), F32),
            pltpu.VMEM((256, 128), F32),
            pltpu.VMEM((SEQ, 128), F32),
            pltpu.VMEM((SEQ, 128), F32),
            pltpu.VMEM((2, SEQ, 128), F32),
            pltpu.VMEM((N, 16, 128), BF16),
            pltpu.VMEM((16, SEQ, D), BF16),
            pltpu.VMEM((16, SEQ, 128), F32),
            pltpu.VMEM((16, SEQ, 128), F32),
            pltpu.VMEM((4, 4, 4, 2, SEQ, D), BF16),
            pltpu.VMEM((2 * HPAD, D), BF16),
            pltpu.VMEM((HPAD, D), BF16),
            pltpu.VMEM((DEN, D), BF16),
            pltpu.VMEM((DEN, D), BF16),
            pltpu.VMEM((DEN, D), BF16),
            pltpu.VMEM((1, D), F32),
            pltpu.VMEM((2, N * SEQ), jnp.int32),
            pltpu.VMEM((2, N * SEQ), F32),
            pltpu.VMEM((N * SEQ, 128), F32),
            pltpu.VMEM((4, 4, 4, 2, SEQ, 2 * HPAD), F32),
            pltpu.VMEM((4, 4, 4, 2, SEQ, HPAD), BF16),
            pltpu.VMEM((4, 4, 4, 2, SEQ, D), BF16),
            pltpu.VMEM((4, 4, 4, SEQ, D), BF16),
            pltpu.VMEM((4, 4, 4, SEQ, D), BF16),
            pltpu.VMEM((3, 4, 4, SEQ, D), BF16),
            pltpu.VMEM((4, 4, SEQ, D), BF16),
            pltpu.VMEM((3, 4, SEQ, D), BF16),
            pltpu.VMEM((4, SEQ, D), BF16),
            pltpu.VMEM((3, SEQ, D), BF16),
            dma((16,)),
            dma((11,)),
            dma,
            dma,
            dma((8,)),
            dma((16,)),
            dma((8,)),
            dma,
            dma((2,)),
            dma((3, 3)),
            dma((3, 3, 3)),
            dma((3,)),
            dma((3, 4)),
            dma((3,)),
            dma((3, 4)),
            dma((3,)),
            dma((3, 3, 4)),
            dma((3, 3)),
            dma((3, 3)),
            dma((3, 3)),
            dma((3, 3)),
        ],
        compiler_params=pltpu.CompilerParams(
            collective_id=0, has_side_effects=True, vmem_limit_bytes=62 * 1024 * 1024
        ),
    )(*operands)


def local(
    tokens, cache_keys, cache_values, cum_gates, lengths, query_weight, key_weight, value_weight,
    forget_weight, out_weight, norm_gain, norm_bias, dense_gate_weight, dense_up_weight,
    dense_down_weight, dense_scale, expert_gate_weight, expert_up_weight, expert_down_weight,
    routes, route_weights,
):
    return step(
        lengths, tokens, query_weight, key_weight, value_weight, forget_weight.T, cache_keys, cache_values,
        jnp.transpose(cum_gates, (0, 2, 1)), out_weight, norm_gain, norm_bias, expert_gate_weight.T,
        expert_up_weight.T, expert_down_weight, dense_gate_weight.T, dense_up_weight.T, dense_down_weight,
        dense_scale.reshape(1, D), routes.T, route_weights.T,
    )


def solution(mesh):
    return jax.shard_map(
        local,
        mesh=mesh,
        in_specs=(
            P("ep", None), P("ep", None, None), P("ep", None, None), P("ep", None, None), P("ep"),
            P(), P(), P(), P(), P("ep", None), P(), P(), P(None, "ep"), P(None, "ep"), P("ep", None),
            P(), P(None, "ep"), P(None, "ep"), P("ep", None), P(), P(),
        ),
        out_specs=P("ep", None),
        check_vma=False,
    )
```

time: 88.3 us -> 76.8 us (0.87)
  Pallas kernels: 86.6 us -> 75.1 us
    pallas_call x2 -> x1, Pallas kernels: 86.6 us -> 75.1 us  [step(): pl.pallas_call(step_kernel, name='step', out_shape=jax.ShapeDtypeStruct((...]
where the time goes in v2:
time: 76.8 us; the launch traced here: 76.5 us
  Pallas kernels  75.1 us (98%)
  local copies, waits for them, and re-layouts  1.38 us (2%)
    pallas_call x1, Pallas kernels, step(): pl.pallas_call(step_kernel, name='step', out_shape=jax.ShapeDtypeStruct((...  75.1 us

profile of v2, /device:TPU:0, one launch (start us, length us, event | category | flops | bytes accessed | tf_op | source)
XLA Modules:
  0.0 76.5 jit_solution(4552653384256587250)
XLA Ops:
  0.0 75.1 %step.1 = bf16[8,2048]{1,0:T(8,128)(2,1)} custom-call(s32[8]{0:T(128)} %len_ref.1, bf16[8,2048]{1,0:T(8,128)(2,1)} %tok_h.1, bf16[2048,2048]{1,0:T(8,128)(2,1)} %wq_h.1, bf16[2048,128]{1,0:T(8,128)(2,1)} %wk_h.1, bf16[2048,128]{1,0:T(8,128)(2,1)} %wv_h.1, bf16[2,2048]{1,0:T(2,128)(2,1)} %bitcast.14, bf16[8,1024,128]{2,1,0:T(8,128)(2,1)} %kc_h.1, ...), custom_call_target="tpu_custom_call" | custom-call | tf_op jit(solution)/shard_map/step/pallas_call | solution.py:417
  75.1 1.4 %copy.23 = bf16[8,2048]{1,0:T(8,128)(2,1)} copy(bf16[8,2048]{1,0:T(8,128)(2,1)} %step.1) | data formatting | bytes 65536

commit v3 on v2

--- a/solution.py
+++ b/solution.py
@@ -21,7 +21,7 @@
 F32 = jnp.float32
 BF16 = jnp.bfloat16
 
-COLOURS = ((0, 768, (2, 1, 0)), (768, 640, (0, 2, 1)), (1408, 640, (1, 0, 2)))
+COLOURS = ((0, 768, (2, 1, 0)), (768, 768, (0, 2, 1)), (1536, 512, (1, 0, 2)))
 
 
 def layer_norm(values, gain_row, shift_row):
@@ -49,7 +49,7 @@
     q3, o3, nk, nv, ng, wbuf, abuf, psend, prec,
     full, wgu, wd, dg, du, dd, scale, routes, shares, portion, acc, hid,
     part, crec, chip, r1, t1, r2, t2, r3,
-    lsem, esem, wsend, wrecv, asend, arecv, fwsend, psem, rsem,
+    lsem, esem, wsend, wrecv, asend, arecv, psem, rsem,
     gsend, grecv, fsend, frecv, csend, crecv, s1send, s1recv, s2send, s2recv, s3send, s3recv,
 ):
     me = lax.axis_index("ep")
@@ -80,13 +80,12 @@
     load("kc", kc_h, kc)
     load("vc", vc_h, vc)
 
+    mates = [group * 16 + lax.rem(slot + k, 16) for k in range(1, 16)]
+    twins = [lax.rem(me + 16 * k, N) for k in range(1, 8)]
+    across = peer_at(1, 3 - 2 * lax.rem(place[1], 2))
     barrier = pltpu.get_barrier_semaphore()
-
-    def hello(i, carry):
-        pl.semaphore_signal(barrier, inc=1, device_id=(lax.rem(me + i, N),), device_id_type=MESH)
-        return carry
-
-    lax.fori_loop(1, N, hello, 0)
+    for peer in twins + mates + [across]:
+        pl.semaphore_signal(barrier, inc=1, device_id=(peer,), device_id_type=MESH)
     later = []
     for src, dst in (
         (gain_h, gain), (bias_h, bias), (eg_h, wgu.at[pl.ds(0, HID)]), (eu_h, wgu.at[pl.ds(HPAD, HID)]),
@@ -129,12 +128,16 @@
     loads["ow"].wait()
     own_w = pltpu.make_async_copy(ow.at[:, pl.ds(pl.multiple_of(slot * 128, 128), 128)], wbuf.at[me], psem)
     own_w.start()
+    pl.semaphore_wait(barrier, 23)
+    for k, peer in enumerate(mates):
+        column = pl.multiple_of(lax.rem(slot + k + 1, 16) * 128, 128)
+        remote(ow.at[:, pl.ds(column, 128)], wbuf.at[me], wsend.at[0], wrecv.at[0], peer).start()
     loads["cg"].wait()
     loads["kc"].wait()
     loads["vc"].wait()
     pos = lax.broadcasted_iota(jnp.int32, (1, SLOTS), 1)
 
-    def sequence(b, carry):
+    def sequence(b):
         used = len_ref[b]
         qb = q3[pl.ds(b, 32, stride=8), :]
         s = lax.dot_general(qb.astype(BF16), kc[b], NT, preferred_element_type=F32)
@@ -154,9 +157,13 @@
         mixed = jnp.dot((e * inv).astype(BF16), vc[b], preferred_element_type=F32)
         mixed = mixed + (eo * inv).astype(BF16).astype(F32) * nv[pl.ds(b, 1), :]
         o3[pl.ds(b, 32, stride=8), :] = mixed
+
+    def sequences(i, carry):
+        for b in range(4):
+            sequence(4 * i + b)
         return carry
 
-    lax.fori_loop(0, SEQ, sequence, 0)
+    lax.fori_loop(0, SEQ // 4, sequences, 0)
     for t in range(16):
         low = o3[(2 * t) * 8:(2 * t + 1) * 8, :]
         high = o3[(2 * t + 1) * 8:(2 * t + 2) * 8, :]
@@ -166,24 +173,15 @@
             low = pltpu.roll(low, 64, 1)
         abuf[slot, :, t * 128:(t + 1) * 128] = jnp.where(lane < 64, low, high).astype(BF16)
 
-    pl.semaphore_wait(barrier, N - 1)
-    sends = []
     for k in range(1, 8):
         other = lax.rem(slot + 2 * k, 16)
-        copy = remote(abuf.at[slot], abuf.at[slot], asend.at[k], arecv.at[k], group * 16 + other)
-        copy.start()
-        sends.append(copy)
-    copy = remote(abuf.at[slot], abuf.at[slot], fwsend.at[0], arecv.at[8], partner)
-    copy.start()
-    sends.append(copy)
-
-    def push(i, carry):
-        peer = lax.rem(me + i, N)
-        column = pl.multiple_of(lax.rem(peer, 16) * 128, 128)
-        remote(ow.at[:, pl.ds(column, 128)], wbuf.at[me], wsend, wrecv, peer).start()
-        return carry
-
-    lax.fori_loop(1, N, push, 0)
+        remote(abuf.at[slot], abuf.at[slot], asend.at[0], arecv.at[k], group * 16 + other).start()
+    remote(abuf.at[slot], abuf.at[slot], asend.at[1], arecv.at[0], partner).start()
+    own_w.wait()
+    wait_bytes(wbuf.at[pl.ds(0, 15)], wrecv.at[0])
+    rows_here = pl.ds(group * 16, 16)
+    for peer in twins:
+        remote(wbuf.at[rows_here], wbuf.at[rows_here], wsend.at[1], wrecv.at[1], peer).start()
 
     for copy in later:
         copy.wait()
@@ -207,13 +205,9 @@
     for k in range(1, 8):
         source = lax.rem(slot + 16 - 2 * k, 16)
         wait_bytes(abuf.at[source], arecv.at[k])
-        copy = remote(abuf.at[source], abuf.at[source], fwsend.at[k], arecv.at[8 + k], partner)
-        copy.start()
-        sends.append(copy)
-    for k in range(8):
-        wait_bytes(abuf.at[slot], arecv.at[8 + k])
-    own_w.wait()
-    wait_bytes(wbuf.at[pl.ds(0, N - 1)], wrecv)
+        remote(abuf.at[source], abuf.at[source], asend.at[1], arecv.at[0], partner).start()
+    wait_bytes(abuf.at[pl.ds(0, 8)], arecv.at[0])
+    wait_bytes(wbuf.at[pl.ds(0, N - 16)], wrecv.at[1])
 
     product = jnp.dot(
         abuf[...].reshape(16 * SEQ, D), wbuf[...].reshape(D, 128), preferred_element_type=F32
@@ -235,64 +229,76 @@
         columns = slice(None) if wide else pl.ds(start, width)
         return ref.at[(*index, *middle, slice(None), columns)]
 
-    def gather_send(colour, phase, fixed):
+    def gather_send(colour, phase, fixed, number=0):
         axis = COLOURS[colour][2][phase]
         view = cut(full, fixed, colour, (core,))
-        for d in (2, 1, 3):
-            remote(view, view, gsend.at[colour, phase], grecv.at[colour, phase, d - 1], peer_at(axis, d)).start()
-
-    def gather_wait(colour, phase, d):
-        order = COLOURS[colour][2]
-        fixed = {a: place[a] for a in order[phase:]}
-        fixed[order[phase]] = lax.rem(place[order[phase]] + 4 - d, 4)
-        wait_bytes(cut(full, fixed, colour, (core,)), grecv.at[colour, phase, d - 1])
-        return fixed
+        for d in (1, 3, 2):
+            remote(
+                view, view, gsend.at[phase], grecv.at[phase if phase < 2 else 2 + number, d - 1], peer_at(axis, d)
+            ).start()
+
+    def gather_wait(phase, d, number=0):
+        wait_bytes(
+            full.at[0, 0, pl.ds(0, 4 if phase else 1), 0], grecv.at[phase if phase < 2 else 2 + number, d - 1]
+        )
+        pieces = []
+        for _, _, order in COLOURS:
+            fixed = {a: place[a] for a in order[phase:]}
+            fixed[order[phase]] = lax.rem(place[order[phase]] + 4 - d, 4)
+            if phase == 2:
+                fixed[order[1]] = lax.rem(place[order[1]] + 4 - number, 4)
+            pieces.append(fixed)
+        return pieces
 
     def forward(colour, fixed, number):
         view = cut(full, fixed, colour, (core,))
-        remote(view, view, fsend.at[colour], frecv.at[colour, number], partner).start()
+        remote(view, view, fsend.at[0], frecv.at[number], partner).start()
+
+    def gather_last(number):
+        for d in (1, 3, 2):
+            for colour, fixed in enumerate(gather_wait(2, d, number)):
+                forward(colour, fixed, number)
+
+    def gate_up(colour, number):
+        start, width, order = COLOURS[colour]
+        fixed = {order[1]: lax.rem(place[order[1]] + 4 - number, 4)}
+        if colour == 0:
+            wait_bytes(full.at[:, :, 0, 0], frecv.at[number])
+        rows = cut(full, fixed, colour, (slice(None),))[...].reshape(256, width)
+        total = cut(acc, fixed, colour, (slice(None),), wide=True)
+        value = total[...].reshape(256, 2 * HPAD) + lax.dot_general(
+            rows, wgu[:, start:start + width], NT, preferred_element_type=F32
+        )
+        total[...] = value.reshape(4, 4, 2, SEQ, 2 * HPAD)
 
     everything = dict(enumerate(place))
     for phase in range(3):
         for colour in range(3):
             gather_send(colour, phase, everything)
     for d in (1, 3, 2):
-        for colour in range(3):
-            fixed = gather_wait(colour, 0, d)
+        for colour, fixed in enumerate(gather_wait(0, d)):
             gather_send(colour, 1, fixed)
             gather_send(colour, 2, fixed)
+    for colour in range(3):
+        order = COLOURS[colour][2]
+        forward(colour, {order[1]: place[order[1]], order[2]: place[order[2]]}, 0)
     for d in (1, 3, 2):
-        for colour in range(3):
-            fixed = gather_wait(colour, 1, d)
-            gather_send(colour, 2, fixed)
+        for colour, fixed in enumerate(gather_wait(1, d)):
+            gather_send(colour, 2, fixed, d)
+            forward(colour, fixed, d)
+    gather_last(0)
     for colour in range(3):
-        last = COLOURS[colour][2][2]
-        forward(colour, {last: place[last]}, 0)
-
-    def gate_up(i, carry):
-        @pl.when(i == 1)
-        def _():
-            for number, d in ((1, 1), (2, 3)):
-                for colour in range(3):
-                    forward(colour, {COLOURS[colour][2][2]: gather_wait(colour, 2, d)[COLOURS[colour][2][2]]}, number)
-
-        @pl.when(i == 2)
-        def _():
-            for colour in range(3):
-                forward(colour, {COLOURS[colour][2][2]: gather_wait(colour, 2, 2)[COLOURS[colour][2][2]]}, 3)
-
-        d = i + (i // 2) * (5 - 2 * i)
-        for colour in range(3):
-            start, width, order = COLOURS[colour]
-            fixed = {order[2]: lax.rem(place[order[2]] + 4 - d, 4)}
-            wait_bytes(cut(full, fixed, colour, (0,)), frecv.at[colour, i])
-            rows = cut(full, fixed, colour, (slice(None),))[...].reshape(256, width)
-            value = lax.dot_general(rows, wgu[:, start:start + width], NT, preferred_element_type=F32)
-            total = cut(acc, fixed, colour, (slice(None),), wide=True)
-            total[...] = total[...] + value.reshape(4, 4, 2, SEQ, 2 * HPAD)
-        return carry
-
-    lax.fori_loop(0, 4, gate_up, 0)
+        gate_up(colour, 0)
+    gather_last(1)
+    gather_last(3)
+    for colour in range(3):
+        gate_up(colour, 1)
+    gate_up(0, 3)
+    gather_last(2)
+    for colour in range(1, 3):
+        gate_up(colour, 3)
+    for colour in range(3):
+        gate_up(colour, 2)
 
     column = lax.broadcasted_iota(jnp.int32, (256, HPAD), 1)
 
@@ -311,104 +317,96 @@
     def turn(i):
         return 2 - i + (i // 2) * (7 - 2 * i)
 
+    def product_of(i, colour):
+        start, width, order = COLOURS[colour]
+        fixed = {order[1]: lax.rem(place[order[1]] + turn(i), 4)}
+        rows = cut(hid, fixed, colour, (slice(None),), wide=True)[...].reshape(256, HPAD)
+        value = jnp.dot(rows, wd[:, start:start + width], preferred_element_type=F32)
+        cut(part, fixed, colour, (slice(None),))[...] = value.astype(BF16).reshape(4, 4, 2, SEQ, width)
+        remote(
+            cut(part, fixed, colour, (1 - core,)), cut(crec, fixed, colour),
+            csend.at[0], crecv.at[colour, i], partner,
+        ).start()
+
+    def join(i, colour):
+        start, width, order = COLOURS[colour]
+        v2 = lax.rem(place[order[1]] + turn(i), 4)
+        fixed = {order[1]: v2}
+        wait_bytes(cut(crec, fixed, colour), crecv.at[colour, i])
+        total = cut(part, fixed, colour, (core,))[...].astype(F32) + cut(crec, fixed, colour)[...].astype(F32)
+        cut(chip, fixed, colour)[...] = total.astype(BF16)
+        for d in (2, 1, 3):
+            remote(
+                cut(chip, {order[2]: lax.rem(place[order[2]] + d, 4), order[1]: v2}, colour),
+                r1.at[d - 1, v2, :, :, pl.ds(start, width)],
+                s1send.at[0], s1recv.at[colour, turn(i)], peer_at(order[2], d),
+            ).start()
+
     def scatter(i, carry):
-        @pl.when(i < 4)
-        def _():
-            for colour in range(3):
-                start, width, order = COLOURS[colour]
-                fixed = {order[2]: lax.rem(place[order[2]] + turn(i), 4)}
-                rows = cut(hid, fixed, colour, (slice(None),), wide=True)[...].reshape(256, HPAD)
-                value = jnp.dot(rows, wd[:, start:start + width], preferred_element_type=F32)
-                cut(part, fixed, colour, (slice(None),))[...] = value.astype(BF16).reshape(4, 4, 2, SEQ, width)
-                remote(
-                    cut(part, fixed, colour, (1 - core,)), cut(crec, fixed, colour),
-                    csend.at[colour], crecv.at[colour, i], partner,
-                ).start()
-
-        @pl.when(i > 0)
-        def _():
-            d = turn(i - 1)
-            for colour in range(3):
-                order = COLOURS[colour][2]
-                v3 = lax.rem(place[order[2]] + d, 4)
-                fixed = {order[2]: v3}
-                wait_bytes(cut(crec, fixed, colour), crecv.at[colour, i - 1])
-                total = cut(part, fixed, colour, (core,))[...].astype(F32) + cut(crec, fixed, colour)[...].astype(F32)
-                cut(chip, fixed, colour)[...] = total.astype(BF16)
-
-                @pl.when(i < 4)
-                def _():
-                    start, width, _ = COLOURS[colour]
-                    for d2 in (2, 1, 3, 0):
-                        v2 = lax.rem(place[order[1]] + d2, 4)
-                        remote(
-                            cut(chip, {order[2]: v3, order[1]: v2}, colour),
-                            r1.at[d - 1, v2, :, :, pl.ds(start, width)],
-                            s1send.at[colour], s1recv.at[colour, d - 1, d2], peer_at(order[2], d),
-                        ).start()
+        for colour in range(3):
+            @pl.when(i < 4)
+            def _(colour=colour):
+                product_of(i, colour)
+
+            @pl.when(i > 0)
+            def _(colour=colour):
+                join(i - 1, colour)
 
         return carry
 
     lax.fori_loop(0, 5, scatter, 0)
-
+    wait_bytes(abuf.at[pl.ds(0, 7)], asend.at[0])
+    wait_bytes(abuf.at[pl.ds(0, 8)], asend.at[1])
+    wait_bytes(psend.at[pl.ds(0, 15)], rsem.at[0])
+    wait_bytes(wbuf.at[pl.ds(0, 15)], wsend.at[0])
+    wait_bytes(wbuf.at[pl.ds(0, N - 16)], wsend.at[1])
+    wait_bytes(full.at[0, 0, pl.ds(0, 3), 0], gsend.at[0])
+    wait_bytes(full.at[0, pl.ds(0, 3), :, 0], gsend.at[1])
+    wait_bytes(full.at[pl.ds(0, 3), :, :, 0], gsend.at[2])
+    wait_bytes(full.at[:, :, :, 0], fsend.at[0])
+    wait_bytes(crec, csend.at[0])
     for d2 in (2, 1, 3, 0):
         for colour in range(3):
             start, width, order = COLOURS[colour]
             columns = pl.ds(start, width)
             v2 = lax.rem(place[order[1]] + d2, 4)
             total = cut(chip, {order[2]: place[order[2]], order[1]: v2}, colour)[...].astype(F32)
-            for d in (2, 1, 3):
-                land = r1.at[d - 1, v2, :, :, columns]
-                wait_bytes(land, s1recv.at[colour, d - 1, d2])
-                total = total + land[...].astype(F32)
+            wait_bytes(r1.at[:, v2, :, :, columns], s1recv.at[colour, d2])
+            for d in range(3):
+                total = total + r1[d, v2, :, :, start:start + width].astype(F32)
             t1[v2, :, :, start:start + width] = total.astype(BF16)
             if d2:
                 remote(
                     t1.at[v2, :, :, columns], r2.at[d2 - 1, :, :, columns],
-                    s2send.at[colour, d2 - 1], s2recv.at[colour, d2 - 1], peer_at(order[1], d2),
+                    s2send.at[0], s2recv.at[colour], peer_at(order[1], d2),
                 ).start()
     for colour in range(3):
         start, width, order = COLOURS[colour]
         columns = pl.ds(start, width)
         total = t1[place[order[1]], :, :, start:start + width].astype(F32)
-        for d in (1, 3, 2):
-            land = r2.at[d - 1, :, :, columns]
-            wait_bytes(land, s2recv.at[colour, d - 1])
-            total = total + land[...].astype(F32)
+        wait_bytes(r2.at[:, :, :, columns], s2recv.at[colour])
+        for d in range(3):
+            total = total + r2[d, :, :, start:start + width].astype(F32)
         t2[:, :, start:start + width] = total.astype(BF16)
         for d in (2, 1, 3):
             remote(
                 t2.at[lax.rem(place[order[0]] + d, 4), :, columns], r3.at[d - 1, :, columns],
-                s3send.at[colour, d - 1], s3recv.at[colour, d - 1], peer_at(order[0], d),
+                s3send.at[0], s3recv.at[colour], peer_at(order[0], d),
             ).start()
+    wait_bytes(r1, s1send.at[0])
+    wait_bytes(r2, s2send.at[0])
     pieces = []
     for colour in range(3):
         start, width, order = COLOURS[colour]
         total = t2[place[order[0]], :, start:start + width].astype(F32)
-        for d in (1, 3, 2):
-            land = r3.at[d - 1, :, pl.ds(start, width)]
-            wait_bytes(land, s3recv.at[colour, d - 1])
-            total = total + land[...].astype(F32)
+        wait_bytes(r3.at[:, :, pl.ds(start, width)], s3recv.at[colour])
+        for d in range(3):
+            total = total + r3[d, :, start:start + width].astype(F32)
         pieces.append(total)
     base = residual_scale * full[place[0], place[1], place[2], core].astype(F32)
     out_ref[...] = layer_norm(base + jnp.concatenate(pieces, axis=-1), gain[1:2, :], bias[1:2, :])
 
-    for copy in sends:
-        copy.wait_send()
-    wait_bytes(psend.at[pl.ds(0, 15)], rsem.at[0])
-    wait_bytes(wbuf.at[pl.ds(0, N - 1)], wsend)
-    for colour in range(3):
-        start, width, order = COLOURS[colour]
-        columns = pl.ds(start, width)
-        wait_bytes(full.at[0, 0, pl.ds(0, 3), 0, :, columns], gsend.at[colour, 0])
-        wait_bytes(full.at[0, pl.ds(0, 3), :, 0, :, columns], gsend.at[colour, 1])
-        wait_bytes(full.at[pl.ds(0, 3), :, :, 0, :, columns], gsend.at[colour, 2])
-        wait_bytes(full.at[:, :, :, 0, :, columns], fsend.at[colour])
-        wait_bytes(crec.at[:, :, :, :, columns], csend.at[colour])
-        wait_bytes(r1.at[:, :, :, :, columns], s1send.at[colour])
-        for d in range(3):
-            wait_bytes(r2.at[d, :, :, columns], s2send.at[colour, d])
-            wait_bytes(r3.at[d, :, columns], s3send.at[colour, d])
+    wait_bytes(r3, s3send.at[0])
 
 
 def step(*operands):
@@ -463,25 +461,24 @@
             pltpu.VMEM((3, SEQ, D), BF16),
             dma((16,)),
             dma((11,)),
-            dma,
-            dma,
-            dma((8,)),
-            dma((16,)),
+            dma((2,)),
+            dma((2,)),
+            dma((2,)),
             dma((8,)),
             dma,
             dma((2,)),
-            dma((3, 3)),
-            dma((3, 3, 3)),
             dma((3,)),
+            dma((6, 3)),
+            dma((1,)),
+            dma((4,)),
+            dma((1,)),
             dma((3, 4)),
+            dma((1,)),
+            dma((3, 4)),
+            dma((1,)),
             dma((3,)),
-            dma((3, 4)),
+            dma((1,)),
             dma((3,)),
-            dma((3, 3, 4)),
-            dma((3, 3)),
-            dma((3, 3)),
-            dma((3, 3)),
-            dma((3, 3)),
         ],
         compiler_params=pltpu.CompilerParams(
             collective_id=0, has_side_effects=True, vmem_limit_bytes=62 * 1024 * 1024

time: 76.8 us -> 71.6 us (0.932)
  Pallas kernels: 75.1 us -> 70 us
    pallas_call x1, Pallas kernels: 75.1 us -> 70 us  [step(): pl.pallas_call(step_kernel, name='step', out_shape=jax.ShapeDtypeStruct((...]
where the time goes in v3:
time: 71.6 us; the launch traced here: 71.4 us
  Pallas kernels  70 us (98%)
  local copies, waits for them, and re-layouts  1.38 us (2%)
    pallas_call x1, Pallas kernels, step(): pl.pallas_call(step_kernel, name='step', out_shape=jax.ShapeDtypeStruct((...  70 us

profile of v3, /device:TPU:0, one launch (start us, length us, event | category | flops | bytes accessed | tf_op | source)
XLA Modules:
  0.0 71.4 jit_solution(11692431618099528204)
XLA Ops:
  0.0 70.0 %step.1 = bf16[8,2048]{1,0:T(8,128)(2,1)} custom-call(s32[8]{0:T(128)} %len_ref.1, bf16[8,2048]{1,0:T(8,128)(2,1)} %tok_h.1, bf16[2048,2048]{1,0:T(8,128)(2,1)} %wq_h.1, bf16[2048,128]{1,0:T(8,128)(2,1)} %wk_h.1, bf16[2048,128]{1,0:T(8,128)(2,1)} %wv_h.1, bf16[2,2048]{1,0:T(2,128)(2,1)} %bitcast.14, bf16[8,1024,128]{2,1,0:T(8,128)(2,1)} %kc_h.1, ...), custom_call_target="tpu_custom_call" | custom-call | tf_op jit(solution)/shard_map/step/pallas_call | solution.py:415
  70.0 1.4 %copy.23 = bf16[8,2048]{1,0:T(8,128)(2,1)} copy(bf16[8,2048]{1,0:T(8,128)(2,1)} %step.1) | data formatting | bytes 65536

commit v4 on v3

--- a/solution.py
+++ b/solution.py
@@ -46,11 +46,11 @@
     eg_h, eu_h, ed_h, dg_h, du_h, dd_h, scale_h, routes_h, shares_h,
     out_ref,
     tok, wq, wk, wv, fw, kc, vc, cg, ow, gain, bias,
-    q3, o3, nk, nv, ng, wbuf, abuf, psend, prec,
+    q3, o3, nk, nv, ng, wpair, wbuf, abuf, psend, prec,
     full, wgu, wd, dg, du, dd, scale, routes, shares, portion, acc, hid,
-    part, crec, chip, r1, t1, r2, t2, r3,
+    part, crec, chip, r1, t1, r2,
     lsem, esem, wsend, wrecv, asend, arecv, psem, rsem,
-    gsend, grecv, fsend, frecv, csend, crecv, s1send, s1recv, s2send, s2recv, s3send, s3recv,
+    gsend, grecv, fsend, frecv, csend, crecv, s1send, s1recv, s2send, s2recv,
 ):
     me = lax.axis_index("ep")
     group = me // 16
@@ -60,8 +60,8 @@
     place = (me // 32, lax.rem(me // 8, 4), lax.rem(me // 2, 4))
     stride = (32, 8, 2)
 
-    def peer_at(axis, d):
-        return me + (lax.rem(place[axis] + d, 4) - place[axis]) * stride[axis]
+    def peer_at(*moves):
+        return me + sum((lax.rem(place[axis] + d, 4) - place[axis]) * stride[axis] for axis, d in moves)
 
     loads = {}
 
@@ -80,12 +80,19 @@
     load("kc", kc_h, kc)
     load("vc", vc_h, vc)
 
-    mates = [group * 16 + lax.rem(slot + k, 16) for k in range(1, 16)]
-    twins = [lax.rem(me + 16 * k, N) for k in range(1, 8)]
-    across = peer_at(1, 3 - 2 * lax.rem(place[1], 2))
     barrier = pltpu.get_barrier_semaphore()
-    for peer in twins + mates + [across]:
+    for peer in [lax.rem(me + 2 * i, N) for i in range(1, N // 2)] + [
+        group * 16 + lax.rem(slot + k, 16) for k in range(1, 16, 2)
+    ]:
         pl.semaphore_signal(barrier, inc=1, device_id=(peer,), device_id_type=MESH)
+    loads["tok"].wait()
+
+    q = jnp.zeros((SEQ, D), F32)
+    for k in range(8):
+        loads[("wq", k)].wait()
+        q = q + jnp.dot(
+            tok[:, k * 256:(k + 1) * 256], wq[k * 256:(k + 1) * 256, :], preferred_element_type=F32
+        )
     later = []
     for src, dst in (
         (gain_h, gain), (bias_h, bias), (eg_h, wgu.at[pl.ds(0, HID)]), (eu_h, wgu.at[pl.ds(HPAD, HID)]),
@@ -95,14 +102,6 @@
         copy = pltpu.make_async_copy(src, dst, esem.at[len(later)])
         copy.start()
         later.append(copy)
-    loads["tok"].wait()
-
-    q = jnp.zeros((SEQ, D), F32)
-    for k in range(8):
-        loads[("wq", k)].wait()
-        q = q + jnp.dot(
-            tok[:, k * 256:(k + 1) * 256], wq[k * 256:(k + 1) * 256, :], preferred_element_type=F32
-        )
     q = q.astype(BF16).astype(F32)
     loads["wk"].wait()
     loads["wv"].wait()
@@ -126,12 +125,9 @@
         q3[h * 8:(h + 1) * 8, :] = jnp.where(keep, tile, 0.0)
 
     loads["ow"].wait()
-    own_w = pltpu.make_async_copy(ow.at[:, pl.ds(pl.multiple_of(slot * 128, 128), 128)], wbuf.at[me], psem)
+    own_columns = pl.ds(pl.multiple_of(slot // 2 * 256, 256), 256)
+    own_w = pltpu.make_async_copy(ow.at[:, own_columns], wpair.at[me // 2], psem)
     own_w.start()
-    pl.semaphore_wait(barrier, 23)
-    for k, peer in enumerate(mates):
-        column = pl.multiple_of(lax.rem(slot + k + 1, 16) * 128, 128)
-        remote(ow.at[:, pl.ds(column, 128)], wbuf.at[me], wsend.at[0], wrecv.at[0], peer).start()
     loads["cg"].wait()
     loads["kc"].wait()
     loads["vc"].wait()
@@ -158,12 +154,23 @@
         mixed = mixed + (eo * inv).astype(BF16).astype(F32) * nv[pl.ds(b, 1), :]
         o3[pl.ds(b, 32, stride=8), :] = mixed
 
+    def push_columns():
+        pl.semaphore_wait(barrier, N // 2 + 7)
+        for i in range(1, N // 2):
+            peer = lax.rem(me + 2 * i, N)
+            columns = pl.ds(pl.multiple_of(lax.rem(peer, 16) // 2 * 256, 256), 256)
+            remote(ow.at[:, columns], wpair.at[me // 2], wsend.at[0], wrecv.at[0], peer).start()
+
     def sequences(i, carry):
-        for b in range(4):
-            sequence(4 * i + b)
+        @pl.when(i == 1)
+        def _():
+            push_columns()
+
+        for b in range(2):
+            sequence(2 * i + b)
         return carry
 
-    lax.fori_loop(0, SEQ // 4, sequences, 0)
+    lax.fori_loop(0, SEQ // 2, sequences, 0)
     for t in range(16):
         low = o3[(2 * t) * 8:(2 * t + 1) * 8, :]
         high = o3[(2 * t + 1) * 8:(2 * t + 2) * 8, :]
@@ -177,12 +184,6 @@
         other = lax.rem(slot + 2 * k, 16)
         remote(abuf.at[slot], abuf.at[slot], asend.at[0], arecv.at[k], group * 16 + other).start()
     remote(abuf.at[slot], abuf.at[slot], asend.at[1], arecv.at[0], partner).start()
-    own_w.wait()
-    wait_bytes(wbuf.at[pl.ds(0, 15)], wrecv.at[0])
-    rows_here = pl.ds(group * 16, 16)
-    for peer in twins:
-        remote(wbuf.at[rows_here], wbuf.at[rows_here], wsend.at[1], wrecv.at[1], peer).start()
-
     for copy in later:
         copy.wait()
     expert = me // 16
@@ -206,8 +207,13 @@
         source = lax.rem(slot + 16 - 2 * k, 16)
         wait_bytes(abuf.at[source], arecv.at[k])
         remote(abuf.at[source], abuf.at[source], asend.at[1], arecv.at[0], partner).start()
+    own_w.wait()
+    wait_bytes(wpair.at[pl.ds(0, N // 2 - 1)], wrecv.at[0])
+    half = pl.ds(pl.multiple_of((1 - core) * 128, 128), 128)
+    remote(wpair.at[:, :, half], wbuf.at[:, core], wsend.at[1], wrecv.at[1], partner).start()
+    wbuf[:, core] = jnp.where(core == 0, wpair[:, :, :128], wpair[:, :, 128:])
     wait_bytes(abuf.at[pl.ds(0, 8)], arecv.at[0])
-    wait_bytes(wbuf.at[pl.ds(0, N - 16)], wrecv.at[1])
+    wait_bytes(wbuf.at[:, 0], wrecv.at[1])
 
     product = jnp.dot(
         abuf[...].reshape(16 * SEQ, D), wbuf[...].reshape(D, 128), preferred_element_type=F32
@@ -229,13 +235,20 @@
         columns = slice(None) if wide else pl.ds(start, width)
         return ref.at[(*index, *middle, slice(None), columns)]
 
-    def gather_send(colour, phase, fixed, number=0):
-        axis = COLOURS[colour][2][phase]
+    everything = dict(enumerate(place))
+
+    def gather_plane(number):
+        for d1 in (0, 1, 3, 2):
+            for colour, (_, _, order) in enumerate(COLOURS):
+                if d1 or number:
+                    view = cut(full, everything, colour, (core,))
+                    where = grecv.at[1, number - 1] if number else grecv.at[0, d1 - 1]
+                    remote(view, view, gsend.at[min(number, 1)], where, peer_at((order[0], d1), (order[1], number))).start()
+
+    def gather_send(colour, fixed, number=0):
         view = cut(full, fixed, colour, (core,))
         for d in (1, 3, 2):
-            remote(
-                view, view, gsend.at[phase], grecv.at[phase if phase < 2 else 2 + number, d - 1], peer_at(axis, d)
-            ).start()
+            remote(view, view, gsend.at[2], grecv.at[2 + number, d - 1], peer_at((COLOURS[colour][2][2], d))).start()
 
     def gather_wait(phase, d, number=0):
         wait_bytes(
@@ -259,44 +272,45 @@
             for colour, fixed in enumerate(gather_wait(2, d, number)):
                 forward(colour, fixed, number)
 
-    def gate_up(colour, number):
+    def gate_up(colour, *numbers):
         start, width, order = COLOURS[colour]
-        fixed = {order[1]: lax.rem(place[order[1]] + 4 - number, 4)}
-        if colour == 0:
-            wait_bytes(full.at[:, :, 0, 0], frecv.at[number])
-        rows = cut(full, fixed, colour, (slice(None),))[...].reshape(256, width)
-        total = cut(acc, fixed, colour, (slice(None),), wide=True)
-        value = total[...].reshape(256, 2 * HPAD) + lax.dot_general(
-            rows, wgu[:, start:start + width], NT, preferred_element_type=F32
+        rows, totals = [], []
+        for number in numbers:
+            fixed = {order[1]: lax.rem(place[order[1]] + 4 - number, 4)}
+            if colour == 0:
+                wait_bytes(full.at[:, :, 0, 0], frecv.at[number])
+            rows.append(cut(full, fixed, colour, (slice(None),))[...].reshape(256, width))
+            totals.append(cut(acc, fixed, colour, (slice(None),), wide=True))
+        value = lax.dot_general(
+            jnp.concatenate(rows, axis=0), wgu[:, start:start + width], NT, preferred_element_type=F32
         )
-        total[...] = value.reshape(4, 4, 2, SEQ, 2 * HPAD)
-
-    everything = dict(enumerate(place))
-    for phase in range(3):
-        for colour in range(3):
-            gather_send(colour, phase, everything)
+        for i, total in enumerate(totals):
+            total[...] = total[...] + value[i * 256:(i + 1) * 256].reshape(4, 4, 2, SEQ, 2 * HPAD)
+
+    for number in (0, 1, 3, 2):
+        gather_plane(number)
+    for colour in range(3):
+        gather_send(colour, everything)
     for d in (1, 3, 2):
         for colour, fixed in enumerate(gather_wait(0, d)):
-            gather_send(colour, 1, fixed)
-            gather_send(colour, 2, fixed)
+            gather_send(colour, fixed)
     for colour in range(3):
         order = COLOURS[colour][2]
         forward(colour, {order[1]: place[order[1]], order[2]: place[order[2]]}, 0)
     for d in (1, 3, 2):
         for colour, fixed in enumerate(gather_wait(1, d)):
-            gather_send(colour, 2, fixed, d)
+            gather_send(colour, fixed, d)
             forward(colour, fixed, d)
     gather_last(0)
-    for colour in range(3):
-        gate_up(colour, 0)
+    gate_up(0, 0)
     gather_last(1)
+    gate_up(1, 0)
     gather_last(3)
-    for colour in range(3):
-        gate_up(colour, 1)
-    gate_up(0, 3)
+    gate_up(2, 0)
+    gate_up(0, 1, 3)
     gather_last(2)
     for colour in range(1, 3):
-        gate_up(colour, 3)
+        gate_up(colour, 1, 3)
     for colour in range(3):
         gate_up(colour, 2)
 
@@ -339,7 +353,7 @@
             remote(
                 cut(chip, {order[2]: lax.rem(place[order[2]] + d, 4), order[1]: v2}, colour),
                 r1.at[d - 1, v2, :, :, pl.ds(start, width)],
-                s1send.at[0], s1recv.at[colour, turn(i)], peer_at(order[2], d),
+                s1send.at[0], s1recv.at[colour, turn(i)], peer_at((order[2], d)),
             ).start()
 
     def scatter(i, carry):
@@ -358,8 +372,8 @@
     wait_bytes(abuf.at[pl.ds(0, 7)], asend.at[0])
     wait_bytes(abuf.at[pl.ds(0, 8)], asend.at[1])
     wait_bytes(psend.at[pl.ds(0, 15)], rsem.at[0])
-    wait_bytes(wbuf.at[pl.ds(0, 15)], wsend.at[0])
-    wait_bytes(wbuf.at[pl.ds(0, N - 16)], wsend.at[1])
+    wait_bytes(wpair.at[pl.ds(0, N // 2 - 1)], wsend.at[0])
+    wait_bytes(wbuf.at[:, 0], wsend.at[1])
     wait_bytes(full.at[0, 0, pl.ds(0, 3), 0], gsend.at[0])
     wait_bytes(full.at[0, pl.ds(0, 3), :, 0], gsend.at[1])
     wait_bytes(full.at[pl.ds(0, 3), :, :, 0], gsend.at[2])
@@ -375,38 +389,25 @@
             for d in range(3):
                 total = total + r1[d, v2, :, :, start:start + width].astype(F32)
             t1[v2, :, :, start:start + width] = total.astype(BF16)
-            if d2:
-                remote(
-                    t1.at[v2, :, :, columns], r2.at[d2 - 1, :, :, columns],
-                    s2send.at[0], s2recv.at[colour], peer_at(order[1], d2),
-                ).start()
-    for colour in range(3):
-        start, width, order = COLOURS[colour]
-        columns = pl.ds(start, width)
-        total = t1[place[order[1]], :, :, start:start + width].astype(F32)
-        wait_bytes(r2.at[:, :, :, columns], s2recv.at[colour])
-        for d in range(3):
-            total = total + r2[d, :, :, start:start + width].astype(F32)
-        t2[:, :, start:start + width] = total.astype(BF16)
-        for d in (2, 1, 3):
-            remote(
-                t2.at[lax.rem(place[order[0]] + d, 4), :, columns], r3.at[d - 1, :, columns],
-                s3send.at[0], s3recv.at[colour], peer_at(order[0], d),
-            ).start()
+            for d1 in (2, 1, 3, 0):
+                if d1 or d2:
+                    remote(
+                        t1.at[v2, lax.rem(place[order[0]] + d1, 4), :, columns], r2.at[4 * d2 + d1, :, columns],
+                        s2send.at[0], s2recv.at[colour], peer_at((order[0], d1), (order[1], d2)),
+                    ).start()
     wait_bytes(r1, s1send.at[0])
-    wait_bytes(r2, s2send.at[0])
     pieces = []
     for colour in range(3):
         start, width, order = COLOURS[colour]
-        total = t2[place[order[0]], :, start:start + width].astype(F32)
-        wait_bytes(r3.at[:, :, pl.ds(start, width)], s3recv.at[colour])
-        for d in range(3):
-            total = total + r3[d, :, start:start + width].astype(F32)
+        total = t1[place[order[1]], place[order[0]], :, start:start + width].astype(F32)
+        wait_bytes(r2.at[pl.ds(1, 15), :, pl.ds(start, width)], s2recv.at[colour])
+        for d in range(1, 16):
+            total = total + r2[d, :, start:start + width].astype(F32)
         pieces.append(total)
     base = residual_scale * full[place[0], place[1], place[2], core].astype(F32)
     out_ref[...] = layer_norm(base + jnp.concatenate(pieces, axis=-1), gain[1:2, :], bias[1:2, :])
 
-    wait_bytes(r3, s3send.at[0])
+    wait_bytes(r2.at[pl.ds(1, 15)], s2send.at[0])
 
 
 def step(*operands):
@@ -435,7 +436,8 @@
             pltpu.VMEM((SEQ, 128), F32),
             pltpu.VMEM((SEQ, 128), F32),
             pltpu.VMEM((2, SEQ, 128), F32),
-            pltpu.VMEM((N, 16, 128), BF16),
+            pltpu.VMEM((N // 2, 16, 256), BF16),
+            pltpu.VMEM((N // 2, 2, 16, 128), BF16),
             pltpu.VMEM((16, SEQ, D), BF16),
             pltpu.VMEM((16, SEQ, 128), F32),
             pltpu.VMEM((16, SEQ, 128), F32),
@@ -456,9 +458,7 @@
             pltpu.VMEM((4, 4, 4, SEQ, D), BF16),
             pltpu.VMEM((3, 4, 4, SEQ, D), BF16),
             pltpu.VMEM((4, 4, SEQ, D), BF16),
-            pltpu.VMEM((3, 4, SEQ, D), BF16),
-            pltpu.VMEM((4, SEQ, D), BF16),
-            pltpu.VMEM((3, SEQ, D), BF16),
+            pltpu.VMEM((16, SEQ, D), BF16),
             dma((16,)),
             dma((11,)),
             dma((2,)),
@@ -477,8 +477,6 @@
             dma((3, 4)),
             dma((1,)),
             dma((3,)),
-            dma((1,)),
-            dma((3,)),
         ],
         compiler_params=pltpu.CompilerParams(
             collective_id=0, has_side_effects=True, vmem_limit_bytes=62 * 1024 * 1024

time: 71.6 us -> 68.8 us (0.961)
  Pallas kernels: 70 us -> 67.2 us
    pallas_call x1, Pallas kernels: 70 us -> 67.2 us  [step(): pl.pallas_call(step_kernel, name='step', out_shape=jax.ShapeDtypeStruct((...]
where the time goes in v4:
time: 68.8 us; the launch traced here: 68.6 us
  Pallas kernels  67.2 us (98%)
  local copies, waits for them, and re-layouts  1.38 us (2%)
    pallas_call x1, Pallas kernels, step(): pl.pallas_call(step_kernel, name='step', out_shape=jax.ShapeDtypeStruct((...  67.2 us

profile of v4, /device:TPU:0, one launch (start us, length us, event | category | flops | bytes accessed | tf_op | source)
XLA Modules:
  0.0 68.6 jit_solution(12240566750528088556)
XLA Ops:
  0.0 67.2 %step.1 = bf16[8,2048]{1,0:T(8,128)(2,1)} custom-call(s32[8]{0:T(128)} %len_ref.1, bf16[8,2048]{1,0:T(8,128)(2,1)} %tok_h.1, bf16[2048,2048]{1,0:T(8,128)(2,1)} %wq_h.1, bf16[2048,128]{1,0:T(8,128)(2,1)} %wk_h.1, bf16[2048,128]{1,0:T(8,128)(2,1)} %wv_h.1, bf16[2,2048]{1,0:T(2,128)(2,1)} %bitcast.14, bf16[8,1024,128]{2,1,0:T(8,128)(2,1)} %kc_h.1, ...), custom_call_target="tpu_custom_call" | custom-call | tf_op jit(solution)/shard_map/step/pallas_call | solution.py:416
  67.2 1.4 %copy.23 = bf16[8,2048]{1,0:T(8,128)(2,1)} copy(bf16[8,2048]{1,0:T(8,128)(2,1)} %step.1) | data formatting | bytes 65536

commit v5 on v4

--- a/solution.py
+++ b/solution.py
@@ -22,6 +22,10 @@
 BF16 = jnp.bfloat16
 
 COLOURS = ((0, 768, (2, 1, 0)), (768, 768, (0, 2, 1)), (1536, 512, (1, 0, 2)))
+
+
+CHIPS = sorted(range(1, N // 2), key=lambda i: -sum(min(i // s % 4, 4 - i // s % 4) for s in (16, 4, 1)))
+MATES = ((0, 1), (0, 3), (1, 0), (0, 2), (1, 1), (1, 3), (1, 2))
 
 
 def layer_norm(values, gain_row, shift_row):
@@ -81,7 +85,7 @@
     load("vc", vc_h, vc)
 
     barrier = pltpu.get_barrier_semaphore()
-    for peer in [lax.rem(me + 2 * i, N) for i in range(1, N // 2)] + [
+    for peer in [lax.rem(me + 2 * i, N) for i in CHIPS] + [
         group * 16 + lax.rem(slot + k, 16) for k in range(1, 16, 2)
     ]:
         pl.semaphore_signal(barrier, inc=1, device_id=(peer,), device_id_type=MESH)
@@ -128,6 +132,14 @@
     own_columns = pl.ds(pl.multiple_of(slot // 2 * 256, 256), 256)
     own_w = pltpu.make_async_copy(ow.at[:, own_columns], wpair.at[me // 2], psem)
     own_w.start()
+    def push_columns():
+        pl.semaphore_wait(barrier, N // 2 + 7)
+        for i in CHIPS:
+            peer = lax.rem(me + 2 * i, N)
+            columns = pl.ds(pl.multiple_of(lax.rem(peer, 16) // 2 * 256, 256), 256)
+            remote(ow.at[:, columns], wpair.at[me // 2], wsend.at[0], wrecv.at[0], peer).start()
+
+    push_columns()
     loads["cg"].wait()
     loads["kc"].wait()
     loads["vc"].wait()
@@ -154,18 +166,7 @@
         mixed = mixed + (eo * inv).astype(BF16).astype(F32) * nv[pl.ds(b, 1), :]
         o3[pl.ds(b, 32, stride=8), :] = mixed
 
-    def push_columns():
-        pl.semaphore_wait(barrier, N // 2 + 7)
-        for i in range(1, N // 2):
-            peer = lax.rem(me + 2 * i, N)
-            columns = pl.ds(pl.multiple_of(lax.rem(peer, 16) // 2 * 256, 256), 256)
-            remote(ow.at[:, columns], wpair.at[me // 2], wsend.at[0], wrecv.at[0], peer).start()
-
     def sequences(i, carry):
-        @pl.when(i == 1)
-        def _():
-            push_columns()
-
         for b in range(2):
             sequence(2 * i + b)
         return carry
@@ -180,9 +181,13 @@
             low = pltpu.roll(low, 64, 1)
         abuf[slot, :, t * 128:(t + 1) * 128] = jnp.where(lane < 64, low, high).astype(BF16)
 
-    for k in range(1, 8):
-        other = lax.rem(slot + 2 * k, 16)
-        remote(abuf.at[slot], abuf.at[slot], asend.at[0], arecv.at[k], group * 16 + other).start()
+    def mate(dy, dx):
+        return lax.rem(slot // 8 + dy, 2) * 8 + lax.rem(place[2] + dx, 4) * 2 + core
+
+    for k, (dy, dx) in enumerate(MATES):
+        remote(
+            abuf.at[slot], abuf.at[slot], asend.at[0], arecv.at[k + 1], group * 16 + mate(dy, dx)
+        ).start()
     remote(abuf.at[slot], abuf.at[slot], asend.at[1], arecv.at[0], partner).start()
     for copy in later:
         copy.wait()
@@ -203,9 +208,9 @@
 
     lax.fori_loop(0, 4, clear, 0)
 
-    for k in range(1, 8):
-        source = lax.rem(slot + 16 - 2 * k, 16)
-        wait_bytes(abuf.at[source], arecv.at[k])
+    for k, (dy, dx) in enumerate(MATES):
+        source = mate(dy, 4 - dx)
+        wait_bytes(abuf.at[source], arecv.at[k + 1])
         remote(abuf.at[source], abuf.at[source], asend.at[1], arecv.at[0], partner).start()
     own_w.wait()
     wait_bytes(wpair.at[pl.ds(0, N // 2 - 1)], wrecv.at[0])

time: 68.8 us -> 67.5 us (0.981)
  Pallas kernels: 67.2 us -> 65.9 us
    pallas_call x1, Pallas kernels: 67.2 us -> 65.9 us  [step(): pl.pallas_call(step_kernel, name='step', out_shape=jax.ShapeDtypeStruct((...]
where the time goes in v5:
time: 67.5 us; the launch traced here: 67.3 us
  Pallas kernels  65.9 us (98%)
  local copies, waits for them, and re-layouts  1.38 us (2%)
    pallas_call x1, Pallas kernels, step(): pl.pallas_call(step_kernel, name='step', out_shape=jax.ShapeDtypeStruct((...  65.9 us
    unnamed x1, local copies, waits for them, and re-layouts  1.38 us

profile of v5, /device:TPU:0, one launch (start us, length us, event | category | flops | bytes accessed | tf_op | source)
XLA Modules:
  0.0 67.3 jit_solution(12841756711246004226)
XLA Ops:
  0.0 65.9 %step.1 = bf16[8,2048]{1,0:T(8,128)(2,1)} custom-call(s32[8]{0:T(128)} %len_ref.1, bf16[8,2048]{1,0:T(8,128)(2,1)} %tok_h.1, bf16[2048,2048]{1,0:T(8,128)(2,1)} %wq_h.1, bf16[2048,128]{1,0:T(8,128)(2,1)} %wk_h.1, bf16[2048,128]{1,0:T(8,128)(2,1)} %wv_h.1, bf16[2,2048]{1,0:T(2,128)(2,1)} %bitcast.14, bf16[8,1024,128]{2,1,0:T(8,128)(2,1)} %kc_h.1, ...), custom_call_target="tpu_custom_call" | custom-call | tf_op jit(solution)/shard_map/step/pallas_call | solution.py:421
  65.9 1.4 %copy.23 = bf16[8,2048]{1,0:T(8,128)(2,1)} copy(bf16[8,2048]{1,0:T(8,128)(2,1)} %step.1) | data formatting | bytes 65536
